TPU v7x, 32 devices: a whole 2x2x4 slice. The times are simulated.
32 devices in a mesh: grp: 2 (over y), sp: 4 (over z), tp: 4 (over x, core).
Axes of the slice: x: 2, y: 2, z: 4, core: 2. Of those that a mesh axis runs over, the one named last changes fastest.
Arguments:
- hidden: bfloat16 [3072, 2048], P(('grp', 'sp'), 'tp'), parts along dimension 0, may hold values from -45 to 45
- norm_gain: bfloat16 [2048], replicated, may hold values from 0.099609375 to 1.8984375
- w_query: bfloat16 [2048, 1024], P(None, 'tp'), may hold values from -0.125 to 0.125
- w_key: bfloat16 [2048, 1024], P(None, 'tp'), may hold values from -0.125 to 0.125
- w_value: bfloat16 [2048, 1024], P(None, 'tp'), may hold values from -0.125 to 0.125
- query_gain: float32 [8, 128], P('tp'), may hold values from 0.3 to 16
- key_gain: float32 [8, 128], P('tp'), may hold values from 0.3 to 16
- w_out: bfloat16 [1024, 2048], P('tp'), may hold values from -1.5 to 1.5
Outputs:
- mixed: bfloat16 [3072, 2048], P(('grp', 'sp'), 'tp'), parts along dimension 0
- log_total: float32 [3072, 8], P(('grp', 'sp'), 'tp'), parts along dimension 0
There are 2 independent parts, one for each index of `grp`. A program takes and returns all parts, laid end to end along the dimension named above; an argument that names none is the same for every part. Nothing has to cross between parts.
All inputs are finite; a program needn't handle non-finite values.
Results may differ from a plain program's by a relative error of at most 0.015.
The roundings to bfloat16 on the way count: a program that leaves them out, or rounds other values in their place, can miss the bound.
Values may be sent and summed in bfloat16 or wider, within the bound.
A program may use at most 64 MiB of HBM per device.

v0:
```python
import math

import jax
import jax.numpy as jnp
from jax import lax
from jax.sharding import PartitionSpec as P

D = 2048
KEYS_BEHIND = 128
MIDDLE_DILATION = 4
WIDEST_DILATION = 16


EPSILON = 1e-06
ROTARY_BASE = 500000.0


def from_behind(value, axis, steps):
    count = lax.axis_size(axis)
    initial, last = (max(0, -steps), min(count, count - steps))
    return lax.ppermute(value, axis, [(source, source + steps) for source in range(initial, last)])


def rotate(values, positions):
    head_width = values.shape[-1]
    inverse = ROTARY_BASE ** (-jnp.arange(0, head_width, 2, dtype=jnp.float32) / head_width)
    angles = positions[:, None] * inverse[None, :]
    cosine = jnp.cos(angles)[:, None, :]
    sine = jnp.sin(angles)[:, None, :]
    half_width = head_width // 2
    first_half = values[..., :half_width]
    second_half = values[..., half_width:]
    return jnp.concatenate(
        [first_half * cosine - second_half * sine, second_half * cosine + first_half * sine],
        axis=-1,
    )


def head_norm(values, gains):
    normed = values * lax.rsqrt(jnp.mean(values * values, axis=-1, keepdims=True) + EPSILON)
    return normed * gains[None, :, :]


def earlier_pairs(own_pair, token_rows):
    distant_shards = (KEYS_BEHIND * WIDEST_DILATION + token_rows - 1) // token_rows
    pieces = [own_pair]
    for distance in range(1, distant_shards + 1):
        pieces.insert(0, from_behind(own_pair, "sp", distance))
    buffer = jnp.concatenate(pieces, axis=1)
    return buffer


def local_branch(query, key_rows, value_rows, dilation_step, first_pos):
    token_rows, head_count, head_width = query.shape
    reach_rows = KEYS_BEHIND * dilation_step
    buffer_rows = key_rows.shape[0]
    class_rows = token_rows // dilation_step
    class_keys = class_rows + KEYS_BEHIND
    window_start = buffer_rows - token_rows - reach_rows
    key_window = key_rows[window_start:]
    value_window = value_rows[window_start:]
    query_class = query.reshape(class_rows, dilation_step, head_count, head_width).transpose(
        1, 0, 2, 3
    )
    key_class = key_window.reshape(class_keys, dilation_step, head_count, head_width).transpose(
        1, 0, 2, 3
    )
    value_class = value_window.reshape(class_keys, dilation_step, head_count, head_width).transpose(
        1, 0, 2, 3
    )
    block_rows = math.gcd(class_rows, KEYS_BEHIND) if class_rows > KEYS_BEHIND else class_rows
    block_count = class_rows // block_rows
    query_blocks = query_class.reshape(
        dilation_step, block_count, block_rows, head_count, head_width
    )
    key_blocks = jnp.stack(
        [
            key_class[:, number * block_rows : number * block_rows + block_rows + KEYS_BEHIND]
            for number in range(block_count)
        ],
        axis=1,
    )
    value_blocks = jnp.stack(
        [
            value_class[:, number * block_rows : number * block_rows + block_rows + KEYS_BEHIND]
            for number in range(block_count)
        ],
        axis=1,
    )
    scores = jnp.einsum(
        "rnqhd,rnkhd->rnhqk", query_blocks, key_blocks, preferred_element_type=jnp.float32
    ) * head_width ** (-0.5)
    row_index = jnp.arange(block_rows, dtype=jnp.int32)[:, None]
    col_index = jnp.arange(block_rows + KEYS_BEHIND, dtype=jnp.int32)[None, :]
    distance = KEYS_BEHIND + row_index - col_index
    in_band = (distance >= 0) & (distance <= KEYS_BEHIND)
    class_index = jnp.arange(block_count, dtype=jnp.int32)[:, None] * block_rows + col_index
    residue = jnp.arange(dilation_step, dtype=jnp.int32)[:, None, None]
    key_position = first_pos - reach_rows + class_index[None] * dilation_step + residue
    allowed = in_band[None, None, None, :, :] & (key_position >= 0)[:, :, None, None, :]
    scores = jnp.where(allowed, scores, -jnp.inf)
    row_max = jnp.max(scores, axis=-1, keepdims=True)
    weights = jnp.exp(scores - row_max)
    weight_sum = jnp.sum(weights, axis=-1)
    weighted = jnp.einsum(
        "rnhqk,rnkhd->rnqhd",
        weights.astype(jnp.bfloat16),
        value_blocks,
        preferred_element_type=jnp.float32,
    )
    branch_out = weighted / jnp.transpose(weight_sum, (0, 1, 3, 2))[..., None]
    branch_out = branch_out.reshape(dilation_step, class_rows, head_count, head_width).transpose(
        1, 0, 2, 3
    )
    branch_out = branch_out.reshape(token_rows, head_count, head_width)
    log_sum = jnp.transpose(row_max[..., 0] + jnp.log(weight_sum), (0, 1, 3, 2))
    log_sum = (
        log_sum.reshape(dilation_step, class_rows, head_count)
        .transpose(1, 0, 2)
        .reshape(token_rows, head_count)
    )
    return (branch_out, log_sum)


def local(hidden, norm_gain, w_query, w_key, w_value, query_gain, key_gain, w_out):
    token_rows = hidden.shape[0]
    local_width = w_query.shape[1]
    head_count = query_gain.shape[0]
    head_width = query_gain.shape[1]
    gain_full = norm_gain.astype(jnp.float32)
    raw_piece = lax.all_gather(hidden, "tp", axis=1, tiled=True).astype(jnp.float32)
    scaled = (raw_piece * gain_full[None, :]).astype(jnp.bfloat16)

    def add_product(weight):
        return jnp.dot(scaled, weight, preferred_element_type=jnp.float32)

    query_raw = add_product(w_query)
    key_raw = add_product(w_key)
    value_raw = add_product(w_value)
    squares = jnp.sum(raw_piece * raw_piece, axis=1)
    row_scale = lax.rsqrt(squares / D + EPSILON)[:, None]
    first_pos = lax.axis_index("sp") * token_rows
    positions = (jnp.arange(token_rows, dtype=jnp.int32) + first_pos).astype(jnp.float32)
    query = rotate(
        head_norm((query_raw * row_scale).reshape(token_rows, head_count, head_width), query_gain),
        positions,
    ).astype(jnp.bfloat16)
    key_now = rotate(
        head_norm((key_raw * row_scale).reshape(token_rows, head_count, head_width), key_gain),
        positions,
    ).astype(jnp.bfloat16)
    value_now = (value_raw * row_scale).astype(jnp.bfloat16)
    own_pair = jnp.stack([key_now.reshape(token_rows, local_width), value_now], axis=0)
    buffer = earlier_pairs(own_pair, token_rows)
    key_rows = buffer[0].reshape(-1, head_count, head_width)
    value_rows = buffer[1].reshape(-1, head_count, head_width)
    branch_outs = []
    branch_logs = []
    for dilation_step in (1, MIDDLE_DILATION, WIDEST_DILATION):
        branch_out, log_sum = local_branch(query, key_rows, value_rows, dilation_step, first_pos)
        branch_outs.append(branch_out)
        branch_logs.append(log_sum)
    stacked_logs = jnp.stack(branch_logs, axis=0)
    peak = jnp.max(stacked_logs, axis=0)
    log_total = peak + jnp.log(jnp.sum(jnp.exp(stacked_logs - peak[None]), axis=0))
    shares = jnp.exp(stacked_logs - log_total[None])
    attended = jnp.sum(shares[..., None] * jnp.stack(branch_outs, axis=0), axis=0)
    attended = attended.astype(jnp.bfloat16).reshape(token_rows, local_width)
    column_block = lax.all_to_all(w_out, "tp", split_axis=1, concat_axis=0, tiled=True)
    mixed = jnp.dot(
        lax.all_gather(attended, "tp", axis=1, tiled=True),
        column_block,
        preferred_element_type=jnp.float32,
    )
    return (mixed.astype(jnp.bfloat16), log_total)


def solution(mesh):
    placed = (
        P(("grp", "sp"), "tp"),
        P(),
        P(None, "tp"),
        P(None, "tp"),
        P(None, "tp"),
        P("tp", None),
        P("tp", None),
        P("tp", None),
    )
    return jax.shard_map(
        local,
        mesh=mesh,
        in_specs=placed,
        out_specs=(P(("grp", "sp"), "tp"), P(("grp", "sp"), "tp")),
        check_vma=False,
    )
```

profile of v0, /device:TPU:17, one launch (start us, length us, event | category | flops | bytes accessed | tf_op | source)
XLA Modules:
  0.0 135.2 jit_solution(7337849643305904054)
XLA Ops:
  7.9 2.3 %copy.167 = bf16[256,2048]{0,1:T(8,128)(2,1)} copy(bf16[256,2048]{1,0:T(8,128)(2,1)} %param.15) | data formatting | bytes 2097152 | tf_op args[7]
  10.2 4.3 %all-to-all-start = ((bf16[256,4,512]{0,2,1:T(8,128)(2,1)}), bf16[256,4,512]{0,2,1:T(8,128)(2,1)S(1)}, u32[]{:S(2)}, u32[]{:S(2)}) async-start(bf16[256,4,512]{0,2,1:T(8,128)(2,1)} %bitcast.65), calls=%async_computation | async-start | bytes 2097152 | tf_op jit(solution)/shard_map/all_to_all | solution.py:169
  16.3 1.4 %multiply_cosine_fusion = (f32[384,64]{1,0:T(8,128)S(1)}, f32[384,64]{1,0:T(8,128)}) fusion(f32[64]{0:T(128)S(1)} %multiply_power_fusion, f32[384]{0:T(512)S(1)} %add_convert_fusion.2), kind=kLoop, calls=%fused_computation.71 | loop fusion | flops 24576 | bytes 198400 | tf_op jit(solution)/shard_map/cos | solution.py:28
  17.8 20.8 %all-gather.2.cloned.1.call-done = bf16[384,2048]{1,0:T(8,128)(2,1)} async-done(((bf16[384,512]{1,0:T(8,128)(2,1)}), bf16[384,2048]{1,0:T(8,128)(2,1)}) %all-gather.2.cloned.1.call-update) | async-done | bytes 1572880 | tf_op jit(solution)/shard_map/all_gather | solution.py:131
  38.6 1.9 %fusion.1 = f32[384]{0:T(512)S(1)} fusion(bf16[384,2048]{1,0:T(8,128)(2,1)} %all-gather.2.cloned.1.call-done), kind=kLoop, calls=%fused_computation.3 | loop fusion | flops 2358912 | bytes 1574400 | tf_op jit(solution)/shard_map/reduce_sum | solution.py:140
  40.5 0.8 multiply_reduce_fusion
  41.5 2.5 %multiply_reduce_fusion.1 = (f32[384,2]{0,1:T(2,128)S(1)}, f32[384,256]{0,1:T(8,128)S(1)}) fusion(f32[384]{0:T(512)S(1)} %add_rsqrt_fusion.2, bf16[2048,256]{1,0:T(8,128)(2,1)} %param.10, bf16[384,2048]{1,0:T(8,128)(2,1)} %all-gather.2.cloned.1.call-done, f32[2048]{0:T(1024)S(1)} %convert_element_type.58), kind=kOutput, calls=%fused_computation.69 | convolution fusion | flops 405306624 | bytes 3027456 | tf_op jit(solution)/shard_map/dot_general | solution.py:135
  44.4 1.3 subtract_convert_fusion.1
  46.0 2.5 %fusion.20 = bf16[1,384,256]{1,2,0:T(8,128)(2,1)S(1)} fusion(bf16[2048,256]{1,0:T(8,128)(2,1)} %param.12, bf16[384,2048]{1,0:T(8,128)(2,1)} %all-gather.2.cloned.1.call-done, f32[2048]{0:T(1024)S(1)} %convert_element_type.58, f32[384]{0:T(512)S(1)} %add_rsqrt_fusion.2), kind=kOutput, calls=%fused_computation.25 | convolution fusion | flops 405209088 | bytes 2827776 | tf_op jit(solution)/shard_map/dot_general | solution.py:135
  48.6 0.8 pad_maximum_fusion.2
  50.1 1.4 %collective-permute-start.3 = (bf16[2,384,256]{1,2,0:T(8,128)(2,1)}, bf16[2,384,256]{1,2,0:T(8,128)(2,1)}, u32[]{:S(2)}, u32[]{:S(2)}) collective-permute-start(bf16[2,384,256]{1,2,0:T(8,128)(2,1)} %pad_maximum_fusion.2), channel_id=1, source_target_pairs={{0,12},{1,13},{2,14},{3,15},{16,28},{17,29},{18,30},{19,31}} | collective-permute-start | bytes 1179656 | tf_op jit(solution)/shard_map/ppermute | solution.py:21
  52.2 1.3 copy.168
  53.5 1.3 collective-permute-start.1
  54.8 3.3 %collective-permute-start = (bf16[2,384,256]{1,2,0:T(8,128)(2,1)}, bf16[2,384,256]{1,2,0:T(8,128)(2,1)S(1)}, u32[]{:S(2)}, u32[]{:S(2)}) collective-permute-start(bf16[2,384,256]{1,2,0:T(8,128)(2,1)} %pad_maximum_fusion.2), channel_id=1, source_target_pairs={{0,4},{4,8},{8,12},{1,5},{5,9},{9,13},{2,6},{6,10},{10,14},{3,7},{... | collective-permute-start | bytes 1179656 | tf_op jit(solution)/shard_map/ppermute | solution.py:21
  58.0 0.7 copy.150
  58.8 0.7 copy.149
  61.1 1.1 constant_dynamic-update-slice_fusion.3
  62.2 10.8 %collective-permute-done.1 = bf16[2,384,256]{1,2,0:T(8,128)(2,1)S(1)} collective-permute-done((bf16[2,384,256]{1,2,0:T(8,128)(2,1)}, bf16[2,384,256]{1,2,0:T(8,128)(2,1)S(1)}, u32[]{:S(2)}, u32[]{:S(2)}) %collective-permute-start.1) | collective-permute-done | bytes 393248 | tf_op jit(solution)/shard_map/ppermute | solution.py:21
  73.0 17.4 %collective-permute-done = bf16[2,384,256]{1,2,0:T(8,128)(2,1)S(1)} collective-permute-done((bf16[2,384,256]{1,2,0:T(8,128)(2,1)}, bf16[2,384,256]{1,2,0:T(8,128)(2,1)S(1)}, u32[]{:S(2)}, u32[]{:S(2)}) %collective-permute-start) | collective-permute-done | bytes 393248 | tf_op jit(solution)/shard_map/ppermute | solution.py:21
  91.5 1.5 %copy.151 = bf16[1,2432,256]{2,1,0:T(8,128)(2,1)} copy(bf16[1,2432,256]{1,2,0:T(8,128)(2,1)S(1)} %get-tuple-element.2) | data formatting | bytes 2490368 | tf_op jit(solution)/shard_map/slice | solution.py:60
  92.9 2.9 %reshape.537 = bf16[152,16,2,128]{3,2,1,0:T(2,128)(2,1)S(1)} reshape(bf16[1,2432,256]{2,1,0:T(8,128)(2,1)} %copy.151) | data formatting | bytes 2490368 | tf_op jit(solution)/shard_map/reshape | solution.py:65
  95.8 2.0 %fusion.85 = (f32[16,2,24]{2,1,0:T(2,128)S(1)}, f32[16,2,24,152]{3,2,1,0:T(8,128)S(1)}) fusion(bf16[152,16,2,128]{3,2,1,0:T(2,128)(2,1)S(1)} %reshape.537, bf16[24,16,2,64]{3,0,2,1:T(8,128)(2,1)} %copy.150, bf16[24,16,2,64]{3,0,2,1:T(8,128)(2,1)} %copy.149, pred[16,24,152]{2,1,0:T(8,128)(4,1)} %broadcast_and_fusion), kind=kOutput, calls=%fused_computation.142 | convolution fusion | flops 30627072 | bytes 1970176 | tf_op jit(solution)/shard_map/rnqhd,rnkhd->rnhqk/dot_general | solution.py:90
  97.8 0.9 copy-done.5
  101.1 2.1 %maximum_maximum_fusion = (bf16[1,896,256]{1,2,0:T(8,128)(2,1)S(1)}, bf16[1,896,256]{1,2,0:T(8,128)(2,1)}) fusion(bf16[1,384,256]{1,2,0:T(8,128)(2,1)} %copy-done.7, bf16[1,384,256]{1,2,0:T(8,128)(2,1)} %bitcast.176, bf16[2,384,256]{1,2,0:T(8,128)(2,1)} %copy-done.3, bf16[2,384,256]{1,2,0:T(8,128)(2,1)} %copy-done.15), kind=kLoop, calls=%fused_computation.43 | loop fusion | flops 3670016 | bytes 2097152 | tf_op jit(solution)/shard_map/slice | solution.py:60
  103.5 1.5 %fusion.86 = (f32[4,2,96]{2,1,0:T(2,128)S(1)}, f32[4,2,96,224]{3,2,1,0:T(8,128)S(1)}) fusion(bf16[224,4,2,128]{3,2,1,0:T(2,128)(2,1)S(1)} %reshape.535, bf16[96,4,2,64]{3,0,2,1:T(8,128)(2,1)S(1)} %copy-done.18, bf16[96,4,2,64]{3,0,2,1:T(8,128)(2,1)} %copy.144, pred[4,96,224]{2,1,0:T(8,128)(4,1)S(1)} %copy-done.20), kind=kOutput, calls=%fused_computation.143 | convolution fusion | flops 44948736 | bytes 1432576 | tf_op jit(solution)/shard_map/rnqhd,rnkhd->rnhqk/dot_general | solution.py:90
  106.1 0.7 stack_reshape.13
  106.8 0.7 stack.53
  107.5 0.8 copy.163
  108.3 1.2 reshape.542
  109.5 2.1 %fusion.29 = f32[24,16,2,128]{3,0,2,1:T(8,128)S(1)} fusion(bf16[152,16,2,128]{3,2,1,0:T(2,128)(2,1)} %reshape.542, f32[16,2,24,152]{3,2,1,0:T(8,128)S(1)} %copy-done.6, f32[16,2,24]{2,1,0:T(2,128)S(1)} %get-tuple-element.26, f32[16,24,2]{1,2,0:T(2,128)} %bitcast.200), kind=kOutput, calls=%fused_computation.30 | convolution fusion | flops 30216192 | bytes 2111488 | tf_op jit(solution)/shard_map/rnhqk,rnkhd->rnqhd/dot_general | solution.py:105
  117.1 8.7 %all_gather.7 = bf16[384,1024]{0,1:T(8,128)(2,1)S(1)} all-gather(bf16[384,256]{0,1:T(8,128)(2,1)S(1)} %bitcast.191), channel_id=1, replica_groups=mesh['grp'=2,'sp'=4,'tp'=4] {'tp'}, dimensions={1}, use_global_device_ids=true | all-gather | bytes 983040 | tf_op jit(solution)/shard_map/all_gather | solution.py:171
  125.8 2.6 %convolution_convert_fusion = bf16[384,512]{1,0:T(8,128)(2,1)} fusion(bf16[384,1024]{0,1:T(8,128)(2,1)S(1)} %all_gather.7, bf16[1024,512]{1,0:T(8,128)(2,1)} %bitcast.190), kind=kOutput, calls=%fused_computation.10 | convolution fusion | flops 402849792 | bytes 2228224 | tf_op jit(solution)/shard_map/dot_general | solution.py:170
  (143 shorter events, 16.5 us)
Async XLA Ops:
  7.2 33.3 %copy-start = (bf16[2048,256]{1,0:T(8,128)(2,1)S(1)}, bf16[2048,256]{1,0:T(8,128)(2,1)}, u32[]{:S(2)}) copy-start(bf16[2048,256]{1,0:T(8,128)(2,1)} %param.11) | copy-start | bytes 3145732
  7.2 31.4 %all-gather.2.cloned.1.call-start = ((), (), s32[]{:S(2)}) async-start(), calls=%async_computation.1 | async-start | bytes 1966080 | tf_op jit(solution)/shard_map/all_gather | solution.py:131
  10.2 4.3 %copy-start.31 = (bf16[2048]{0:T(1024)(128)(2,1)S(1)}, bf16[2048]{0:T(1024)(128)(2,1)}, u32[]{:S(2)}) copy-start(bf16[2048]{0:T(1024)(128)(2,1)} %param.9) | copy-start | bytes 12292
  10.2 42.0 %all-to-all-start = ((bf16[256,4,512]{0,2,1:T(8,128)(2,1)}), bf16[256,4,512]{0,2,1:T(8,128)(2,1)S(1)}, u32[]{:S(2)}, u32[]{:S(2)}) async-start(bf16[256,4,512]{0,2,1:T(8,128)(2,1)} %bitcast.65), calls=%async_computation | async-start | bytes 2097152 | tf_op jit(solution)/shard_map/all_to_all | solution.py:169
  38.5 1.9 %copy-start.14 = (bf16[384,2048]{1,0:T(8,128)(2,1)S(1)}, bf16[384,2048]{1,0:T(8,128)(2,1)}, u32[]{:S(2)}) copy-start(bf16[384,2048]{1,0:T(8,128)(2,1)} %all-gather.2.cloned.1.call-done) | copy-start | bytes 4718596
  41.5 2.7 %copy-start.32 = (f32[2,128]{1,0:T(2,128)S(1)}, f32[2,128]{1,0:T(2,128)}, u32[]{:S(2)}) copy-start(f32[2,128]{1,0:T(2,128)} %param.14) | copy-start | bytes 3076
  41.5 2.7 %copy-start.33 = (f32[2,128]{1,0:T(2,128)S(1)}, f32[2,128]{1,0:T(2,128)}, u32[]{:S(2)}) copy-start(f32[2,128]{1,0:T(2,128)} %param.13) | copy-start | bytes 3076
  45.7 13.8 %copy-start.12 = (bf16[384,2,64]{2,0,1:T(8,128)(2,1)}, bf16[384,2,64]{2,0,1:T(8,128)(2,1)S(1)}, u32[]{:S(2)}) copy-start(bf16[384,2,64]{2,0,1:T(8,128)(2,1)S(1)} %get-tuple-element.9) | copy-start | bytes 294916
  45.7 14.5 %copy-start.10 = (bf16[384,2,64]{2,0,1:T(8,128)(2,1)}, bf16[384,2,64]{2,0,1:T(8,128)(2,1)S(1)}, u32[]{:S(2)}) copy-start(bf16[384,2,64]{2,0,1:T(8,128)(2,1)S(1)} %get-tuple-element.8) | copy-start | bytes 294916
  46.0 44.5 %copy-start.1 = (bf16[384,2,128]{0,2,1:T(8,128)(2,1)}, bf16[384,2,128]{0,2,1:T(8,128)(2,1)S(1)}, u32[]{:S(2)}) copy-start(bf16[384,2,128]{0,2,1:T(8,128)(2,1)S(1)} %copy.139) | copy-start | bytes 589828
  48.6 42.0 %copy-start.7 = (bf16[1,384,256]{1,2,0:T(8,128)(2,1)}, bf16[1,384,256]{1,2,0:T(8,128)(2,1)S(1)}, u32[]{:S(2)}) copy-start(bf16[1,384,256]{1,2,0:T(8,128)(2,1)S(1)} %fusion.20) | copy-start | bytes 589828
  49.4 11.5 %collective-permute-start.2 = (bf16[2,384,256]{1,2,0:T(8,128)(2,1)}, bf16[2,384,256]{1,2,0:T(8,128)(2,1)S(1)}, u32[]{:S(2)}, u32[]{:S(2)}) collective-permute-start(bf16[2,384,256]{1,2,0:T(8,128)(2,1)} %pad_maximum_fusion.2), channel_id=1, source_target_pairs={} | collective-permute-start | bytes 1179656 | tf_op jit(solution)/shard_map/ppermute | solution.py:21
  50.1 11.0 %collective-permute-start.3 = (bf16[2,384,256]{1,2,0:T(8,128)(2,1)}, bf16[2,384,256]{1,2,0:T(8,128)(2,1)}, u32[]{:S(2)}, u32[]{:S(2)}) collective-permute-start(bf16[2,384,256]{1,2,0:T(8,128)(2,1)} %pad_maximum_fusion.2), channel_id=1, source_target_pairs={{0,12},{1,13},{2,14},{3,15},{16,28},{17,29},{18,30},{19,31}} | collective-permute-start | bytes 1179656 | tf_op jit(solution)/shard_map/ppermute | solution.py:21
  53.5 19.5 %collective-permute-start.1 = (bf16[2,384,256]{1,2,0:T(8,128)(2,1)}, bf16[2,384,256]{1,2,0:T(8,128)(2,1)S(1)}, u32[]{:S(2)}, u32[]{:S(2)}) collective-permute-start(bf16[2,384,256]{1,2,0:T(8,128)(2,1)} %pad_maximum_fusion.2), channel_id=1, source_target_pairs={{0,8},{4,12},{1,9},{5,13},{2,10},{6,14},{3,11},{7,15},{16,24},{20,... | collective-permute-start | bytes 1179656 | tf_op jit(solution)/shard_map/ppermute | solution.py:21
  54.8 35.7 %collective-permute-start = (bf16[2,384,256]{1,2,0:T(8,128)(2,1)}, bf16[2,384,256]{1,2,0:T(8,128)(2,1)S(1)}, u32[]{:S(2)}, u32[]{:S(2)}) collective-permute-start(bf16[2,384,256]{1,2,0:T(8,128)(2,1)} %pad_maximum_fusion.2), channel_id=1, source_target_pairs={{0,4},{4,8},{8,12},{1,5},{5,9},{9,13},{2,6},{6,10},{10,14},{3,7},{... | collective-permute-start | bytes 1179656 | tf_op jit(solution)/shard_map/ppermute | solution.py:21
  73.0 17.6 %copy-start.15 = (bf16[2,384,256]{1,2,0:T(8,128)(2,1)}, bf16[2,384,256]{1,2,0:T(8,128)(2,1)S(1)}, u32[]{:S(2)}) copy-start(bf16[2,384,256]{1,2,0:T(8,128)(2,1)S(1)} %collective-permute-done.1) | copy-start | bytes 1179652
  101.1 2.5 %copy-start.18 = (bf16[96,4,2,64]{3,0,2,1:T(8,128)(2,1)S(1)}, bf16[96,4,2,64]{3,0,2,1:T(8,128)(2,1)}, u32[]{:S(2)}) copy-start(bf16[96,4,2,64]{3,0,2,1:T(8,128)(2,1)} %copy.145) | copy-start | bytes 294916
  101.1 2.5 %copy-start.20 = (pred[4,96,224]{2,1,0:T(8,128)(4,1)S(1)}, pred[4,96,224]{2,1,0:T(8,128)(4,1)}, u32[]{:S(2)}) copy-start(pred[4,96,224]{2,1,0:T(8,128)(4,1)} %broadcast_and_fusion.1) | copy-start | bytes 258052
  105.0 2.5 %copy-start.24 = (f32[4,2,96]{2,1,0:T(2,128)}, f32[4,2,96]{2,1,0:T(2,128)S(1)}, u32[]{:S(2)}) copy-start(f32[4,2,96]{2,1,0:T(2,128)S(1)} %get-tuple-element.28) | copy-start | bytes 9220
  105.9 1.6 %copy-start.26 = (f32[4,2,96]{2,1,0:T(2,128)}, f32[4,2,96]{2,1,0:T(2,128)S(1)}, u32[]{:S(2)}) copy-start(f32[4,2,96]{2,1,0:T(2,128)S(1)} %fusion.35) | copy-start | bytes 9220
  108.2 1.3 copy-start.6
  109.5 2.2 %copy-start.9 = (bf16[1,896,256]{1,2,0:T(8,128)(2,1)S(1)}, bf16[1,896,256]{1,2,0:T(8,128)(2,1)}, u32[]{:S(2)}) copy-start(bf16[1,896,256]{1,2,0:T(8,128)(2,1)} %get-tuple-element.5) | copy-start | bytes 1376260
  111.6 1.1 copy-start.17
  111.6 1.1 copy-start.25
  111.6 1.1 copy-start.27
  112.7 0.9 copy-start.2
  112.7 1.1 copy-start.4
  112.7 1.1 copy-start.8
  113.9 0.9 copy-start.11
  113.9 1.0 copy-start.13
  113.9 1.1 copy-start.19
  116.5 11.9 %copy-start.30 = (f32[384,2]{0,1:T(2,128)}, f32[384,2]{0,1:T(2,128)S(1)}, u32[]{:S(2)}) copy-start(f32[384,2]{0,1:T(2,128)S(1)} %log_add_fusion) | copy-start | bytes 9220
  (8 other events, 5.9 us)
Sparse Core Ops, SparseCore 0:
  9.5 28.9 all-gather.1
where the time goes:
time: 136 us; the launch traced here: 135 us
  waiting for transfers between devices  49.7 us (37%)
  local copies, waits for them, and re-layouts  23.9 us (18%)
  matrix products  15.2 us (11%)
  between operations  14.8 us (11%)
  other arithmetic  12 us (9%)
  starting transfers between devices  11 us (8%)
  blocking collectives  8.71 us (6%)
    ppermute x4, waiting for transfers between devices, from_behind(): lax.ppermute(value, axis, [(source, source + steps) for source in range(i...  28.2 us
    all_gather x1, waiting for transfers between devices, local(): lax.all_gather(hidden, 'tp', axis=1, tiled=True).astype(jnp.float32)  20.8 us
    all_gather x1, blocking collectives, local(): lax.all_gather(attended, 'tp', axis=1, tiled=True)  8.71 us
    unnamed x81, local copies, waits for them, and re-layouts  8.5 us
    ppermute x4, starting transfers between devices, from_behind(): lax.ppermute(value, axis, [(source, source + steps) for source in range(i...  6.63 us
    dot_general x3, matrix products, add_product(): return jnp.dot(scaled, weight, preferred_element_type=jnp.float32)  5.79 us
    all_to_all x1, starting transfers between devices, local(): lax.all_to_all(w_out, 'tp', split_axis=1, concat_axis=0, tiled=True)  4.29 us
    dot_general x3, matrix products, local_branch(): jnp.einsum('rnqhd,rnkhd->rnhqk', query_blocks, key_blocks, preferred_elem...  3.85 us
  transfers between devices with their start and end apart: 6, of which 3 were waited for; matrix products, arithmetic and copies ran while one was open for 16% of the time, Pallas kernels for 0%

commit v1 on v0

--- a/solution.py
+++ b/solution.py
@@ -1,8 +1,12 @@
+import functools
 import math
 
 import jax
 import jax.numpy as jnp
+import numpy as np
 from jax import lax
+from jax.experimental import pallas as pl
+from jax.experimental.pallas import tpu as pltpu
 from jax.sharding import PartitionSpec as P
 
 D = 2048
@@ -175,7 +179,364 @@
     return (mixed.astype(jnp.bfloat16), log_total)
 
 
+MESH = pl.DeviceIdType.MESH
+LANES = 128
+
+
+def rotary_table(classes, rows, head_width):
+    inverse = (ROTARY_BASE ** (-np.arange(0, head_width, 2, dtype=np.float64) / head_width)).astype(np.float32)
+    positions = np.arange(classes * classes * rows, dtype=np.float32)
+    angles = (positions[:, None] * inverse[None, :]).astype(np.float64)
+    cosine, sine = np.cos(angles), np.sin(angles)
+    table = np.concatenate([cosine, cosine, -sine, sine], axis=1).astype(np.float32)
+    return table.reshape(classes, rows, classes, 2 * head_width).transpose(0, 2, 1, 3)
+
+
+def class_kernel(
+    hid_ref, gain_ref, qgain_ref, kgain_ref, wq_ref, wk_ref, wv_ref, wo_ref, table_ref,
+    mixed_ref, total_ref,
+    hb, hc, wall, wo, tb, tc, acc_b, acc_c, q_b, kv_b, kv_c, q_c, halo, oc, lsend, ro, rl, at,
+    loc, zs, zr, axs, axr, acs, acr, afs, afr, cxs, cxr, ccs, ccr, cfs, cfr,
+    wos, wor, hs, hr, rs, rr, ls, lr, gxs, gxr, gcs, gcr, gfs, gfr,
+):
+    f32, bf16 = jnp.float32, jnp.bfloat16
+    s, p = lax.axis_index("sp"), lax.axis_index("tp")
+    n = MIDDLE_DILATION
+    rows, width = hid_ref.shape
+    sub = rows // n
+    heads, hd = qgain_ref.shape
+    lw = heads * hd
+    halo_sub = halo.shape[1]
+    halo_rows = n * halo_sub
+    core = p + 1 - 2 * lax.rem(p, 2)
+    xp = lax.rem(p + 2, 4)
+    diag = lax.rem(core + 2, 4)
+
+    def tp_copy(src, dst, ss, sr, q):
+        return pltpu.make_async_remote_copy(
+            src_ref=src, dst_ref=dst, send_sem=ss, recv_sem=sr, device_id={"tp": q}, device_id_type=MESH
+        )
+
+    def sp_copy(src, dst, ss, sr, q):
+        return pltpu.make_async_remote_copy(
+            src_ref=src, dst_ref=dst, send_sem=ss, recv_sem=sr, device_id={"sp": q}, device_id_type=MESH
+        )
+
+    barrier = pltpu.get_barrier_semaphore()
+    for q in (core, xp, diag):
+        pl.semaphore_signal(barrier, inc=1, device_id={"tp": q}, device_id_type=MESH)
+    for k in range(1, n):
+        pl.semaphore_signal(barrier, inc=1, device_id={"sp": lax.rem(s + k, n)}, device_id_type=MESH)
+    loads = [
+        pltpu.make_async_copy(wq_ref, wall.at[:, pl.ds(0, lw)], loc.at[0]),
+        pltpu.make_async_copy(wk_ref, wall.at[:, pl.ds(lw, lw)], loc.at[1]),
+        pltpu.make_async_copy(wv_ref, wall.at[:, pl.ds(2 * lw, lw)], loc.at[2]),
+        pltpu.make_async_copy(table_ref.at[s], tb, loc.at[3]),
+        pltpu.make_async_copy(table_ref.at[:, s], tc, loc.at[4]),
+        pltpu.make_async_copy(
+            wo_ref.at[:, pl.ds(pl.multiple_of(p * width, LANES), width)], wo.at[p], loc.at[5]
+        ),
+    ]
+    for load in loads:
+        load.start()
+
+    def iota(shape, dim):
+        return lax.broadcasted_iota(jnp.int32, shape, dim)
+
+    def row_of(r, part):
+        return n * lax.rem(r, part) + r // part
+
+    square = (rows, rows)
+    to_class = (row_of(iota(square, 0), sub) == iota(square, 1)).astype(f32).astype(bf16)
+    permuted = jnp.dot(to_class, hid_ref[...], preferred_element_type=f32).astype(bf16)
+    hb[p] = permuted.reshape(n, sub, width)
+    hc[p, s] = hb[p, s]
+    pl.semaphore_wait(barrier, 3 + n - 1)
+
+    sends = []
+
+    def go(copy):
+        copy.start()
+        sends.append(copy)
+        return copy
+
+    za = [None] + [
+        go(sp_copy(hb.at[p, lax.rem(s + k, n)], hc.at[p, s], zs.at[k], zr.at[k], lax.rem(s + k, n)))
+        for k in range(1, n)
+    ]
+    ax = [go(tp_copy(hb.at[p, i], hb.at[p, i], axs.at[i], axr.at[i], xp)) for i in range(n)]
+    ac = go(tp_copy(hb.at[p], hb.at[p], acs, acr, core))
+
+    block_of = [lax.rem(s + n - k, n) for k in range(n)]
+    cx, cc = [], []
+
+    def spread(k):
+        piece = hc.at[p, block_of[k]]
+        cx.append(go(tp_copy(piece, piece, cxs.at[k], cxr.at[k], xp)))
+        cc.append(go(tp_copy(piece, piece, ccs.at[k], ccr.at[k], core)))
+
+    spread(0)
+
+    def chunk(source, q):
+        raw = source[q].reshape(rows, width).astype(f32)
+        scaled = (raw * gain_ref[q]).astype(bf16)
+        w = wall[pl.ds(pl.multiple_of(q * width, LANES), width), :]
+        return jnp.dot(scaled, w, preferred_element_type=f32), jnp.sum(raw * raw, axis=1, keepdims=True)
+
+    for load in loads:
+        load.wait()
+    acc_b[...], sq_b = chunk(hb, p)
+    ac.wait_recv()
+    prod, more = chunk(hb, core)
+    acc_b[...] += prod
+    sq_b += more
+
+    af = []
+    for i in range(n):
+        ax[i].wait_recv()
+        af.append(go(tp_copy(hb.at[xp, i], hb.at[xp, i], afs.at[i], afr.at[i], core)))
+        if i >= 1:
+            za[i].wait_recv()
+            spread(i)
+    w_sends = []
+    for j, q in enumerate((core, xp, diag)):
+        w_sends.append(
+            go(tp_copy(wo_ref.at[:, pl.ds(pl.multiple_of(q * width, LANES), width)], wo.at[p], wos.at[j], wor.at[j], q))
+        )
+
+    prod, more = chunk(hb, xp)
+    acc_b[...] += prod
+    sq_b += more
+    for copy in af:
+        copy.wait_recv()
+    prod, more = chunk(hb, diag)
+    sq_b += more
+
+    def finish(acc, sq, table, q_out, kv_out):
+        raw = acc * lax.rsqrt(sq / (width * 4) + EPSILON)
+        table = table[...].reshape(rows, 2 * hd)
+        cosine, sine = table[:, :hd], table[:, hd:]
+        for h in range(heads):
+            for start, gains, out in ((0, qgain_ref, q_out), (lw, kgain_ref, kv_out)):
+                x = raw[:, start + h * hd : start + (h + 1) * hd]
+                x = x * lax.rsqrt(jnp.mean(x * x, axis=-1, keepdims=True) + EPSILON)
+                x = x * gains[pl.ds(h, 1), :]
+                x = x * cosine + pltpu.roll(x, hd // 2, 1) * sine
+                out[:, :, h * hd : (h + 1) * hd] = x.astype(bf16).reshape(n, sub, hd)
+        kv_out[:, :, lw:] = raw[:, 2 * lw :].astype(bf16).reshape(n, sub, lw)
+
+    finish(acc_b[...] + prod, sq_b, tb, q_b, kv_b)
+    halo_send = sp_copy(kv_b.at[:, pl.ds(sub - halo_sub, halo_sub), :], halo, hs, hr, lax.rem(s + 1, n))
+
+    @pl.when(s < n - 1)
+    def _():
+        halo_send.start()
+
+    @pl.when(s == 0)
+    def _():
+        halo[...] = jnp.zeros_like(halo)
+
+    cf = []
+    for k in range(n):
+        cx[k].wait_recv()
+        piece = hc.at[xp, block_of[k]]
+        cf.append(go(tp_copy(piece, piece, cfs.at[k], cfr.at[k], core)))
+        if k == n - 2:
+            for copy in cc:
+                copy.wait_recv()
+            prod, sq_c = chunk(hc, p)
+            prod2, more = chunk(hc, core)
+            acc_c[...] = prod + prod2
+            sq_c += more
+    prod, more = chunk(hc, xp)
+    acc_c[...] += prod
+    sq_c += more
+    for copy in cf:
+        copy.wait_recv()
+    prod, more = chunk(hc, diag)
+    sq_c += more
+    finish(acc_c[...] + prod, sq_c, tc, q_c, kv_c)
+
+    def attend(q, k, v, bias):
+        score = lax.dot_general(q, k, (((1,), (1,)), ((), ())), preferred_element_type=f32)
+        score = score * hd ** (-0.5) + bias
+        top = jnp.max(score, axis=-1, keepdims=True)
+        weight = jnp.exp(score - top)
+        total = jnp.sum(weight, axis=-1, keepdims=True)
+        out = jnp.dot(weight.astype(bf16), v, preferred_element_type=f32) / total
+        return out, top + jnp.log(total)
+
+    behind = iota(square, 0) - iota(square, 1)
+    stride = WIDEST_DILATION // n
+    near = (behind >= 0) & (behind <= KEYS_BEHIND)
+    far = (behind >= 0) & (behind <= KEYS_BEHIND * stride) & ((behind + rows * stride) % stride == 0)
+    bias_c = jnp.where(
+        near & far, math.log(2.0), jnp.where(near | far, 0.0, -jnp.inf)
+    ).astype(f32)
+    lane = iota((rows, LANES), 1)
+    logs = jnp.zeros((rows, LANES), f32)
+    for h in range(heads):
+        cols = slice(h * hd, (h + 1) * hd)
+        vcols = slice(lw + h * hd, lw + (h + 1) * hd)
+        out, lse = attend(
+            q_c[:, :, cols].reshape(rows, hd), kv_c[:, :, cols].reshape(rows, hd),
+            kv_c[:, :, vcols].reshape(rows, hd), bias_c,
+        )
+        oc[:, :, cols] = out.astype(bf16).reshape(n, sub, hd)
+        logs = jnp.where(lane == h, lse, logs)
+    pad = LANES - sub
+    for b in range(n):
+        part = jnp.concatenate([logs[b * sub : (b + 1) * sub], jnp.zeros((pad, LANES), f32)], axis=0)
+        lsend[b] = jnp.transpose(part)[:8]
+    back, back_l = [], []
+    for k in range(1, n):
+        to = lax.rem(s + k, n)
+        back.append(go(sp_copy(oc.at[to], ro.at[s], rs.at[k], rr.at[k], to)))
+        back_l.append(go(sp_copy(lsend.at[to], rl.at[s], ls.at[k], lr.at[k], to)))
+    ro[s] = oc[s]
+    rl[s] = lsend[s]
+
+    @pl.when(s > 0)
+    def _():
+        halo_send.wait_recv()
+
+    total_keys = rows + halo_rows
+    wide = (rows, total_keys)
+    key = iota(wide, 1)
+    key_row = jnp.where(key < rows, row_of(key, sub), row_of(key - rows, halo_sub) - halo_rows)
+    behind = row_of(iota(wide, 0), sub) - key_row
+    ok = (behind >= 0) & (behind <= KEYS_BEHIND) & (key_row + s * rows >= 0)
+    bias_b = jnp.where(ok, 0.0, -jnp.inf).astype(f32)
+    near_parts = []
+    for h in range(heads):
+        cols = slice(h * hd, (h + 1) * hd)
+        vcols = slice(lw + h * hd, lw + (h + 1) * hd)
+        near_parts.append(attend(
+            q_b[:, :, cols].reshape(rows, hd),
+            jnp.concatenate([kv_b[:, :, cols].reshape(rows, hd), halo[:, :, cols].reshape(halo_rows, hd)], axis=0),
+            jnp.concatenate([kv_b[:, :, vcols].reshape(rows, hd), halo[:, :, vcols].reshape(halo_rows, hd)], axis=0),
+            bias_b,
+        ))
+
+    for copy in back + back_l:
+        copy.wait_recv()
+    far_logs = jnp.concatenate(
+        [
+            jnp.transpose(jnp.concatenate([rl[i], jnp.zeros((LANES - 8, LANES), f32)], axis=0))[:sub]
+            for i in range(n)
+        ],
+        axis=0,
+    )
+    logs = jnp.zeros((rows, LANES), f32)
+    mixed_heads = []
+    for h in range(heads):
+        out, lse = near_parts[h]
+        far_lse = far_logs[:, h : h + 1]
+        far_out = ro[:, :, h * hd : (h + 1) * hd].reshape(rows, hd).astype(f32)
+        top = jnp.maximum(lse, far_lse)
+        e_near, e_far = jnp.exp(lse - top), jnp.exp(far_lse - top)
+        both = e_near + e_far
+        logs = jnp.where(lane == h, top + jnp.log(both), logs)
+        mixed_heads.append(((e_near * out + e_far * far_out) / both).astype(bf16))
+    attended = jnp.concatenate(mixed_heads, axis=1)
+    from_class = (iota(square, 0) == row_of(iota(square, 1), sub)).astype(f32).astype(bf16)
+    at[p] = jnp.dot(from_class, attended, preferred_element_type=f32).astype(bf16)
+    half = rows // 2
+    gx = [
+        go(tp_copy(at.at[p, pl.ds(i * half, half)], at.at[p, pl.ds(i * half, half)], gxs.at[i], gxr.at[i], xp))
+        for i in range(2)
+    ]
+    gc = go(tp_copy(at.at[p], at.at[p], gcs, gcr, core))
+    high = logs.astype(bf16)
+    rest = logs - high.astype(f32)
+    middle = rest.astype(bf16)
+    low = (rest - middle.astype(f32)).astype(bf16)
+    ordered = sum(jnp.dot(from_class, x, preferred_element_type=f32) for x in (high, middle, low))
+    total_ref[...] = ordered[:, :heads]
+
+    result = jnp.dot(at[p], wo[p], preferred_element_type=f32)
+    for copy in w_sends:
+        copy.wait_recv()
+    gc.wait_recv()
+    result += jnp.dot(at[core], wo[core], preferred_element_type=f32)
+    gf = []
+    for i in range(2):
+        gx[i].wait_recv()
+        piece = at.at[xp, pl.ds(i * half, half)]
+        gf.append(go(tp_copy(piece, piece, gfs.at[i], gfr.at[i], core)))
+    result += jnp.dot(at[xp], wo[xp], preferred_element_type=f32)
+    for copy in gf:
+        copy.wait_recv()
+    result += jnp.dot(at[diag], wo[diag], preferred_element_type=f32)
+    mixed_ref[...] = result.astype(bf16)
+    for copy in sends:
+        copy.wait_send()
+
+    @pl.when(s < n - 1)
+    def _():
+        halo_send.wait_send()
+
+
+def local_by_class(hidden, norm_gain, w_query, w_key, w_value, query_gain, key_gain, w_out):
+    n = MIDDLE_DILATION
+    rows, width = hidden.shape
+    heads, hd = query_gain.shape
+    lw = heads * hd
+    sub = rows // n
+    halo_sub = KEYS_BEHIND // n
+    bf16, f32 = jnp.bfloat16, jnp.float32
+    table = jnp.asarray(rotary_table(n, sub, hd))
+    vmem = pl.BlockSpec(memory_space=pltpu.VMEM)
+    anyspace = pl.BlockSpec(memory_space=pl.ANY)
+    dma = pltpu.SemaphoreType.DMA
+    return pl.pallas_call(
+        class_kernel,
+        out_shape=(
+            jax.ShapeDtypeStruct((rows, w_out.shape[1] // 4), bf16),
+            jax.ShapeDtypeStruct((rows, heads), f32),
+        ),
+        in_specs=[vmem] * 4 + [anyspace] * 5,
+        out_specs=(vmem, vmem),
+        scratch_shapes=[
+            pltpu.VMEM((4, n, sub, width), bf16),
+            pltpu.VMEM((4, n, sub, width), bf16),
+            pltpu.VMEM((4 * width, 3 * lw), bf16),
+            pltpu.VMEM((4, lw, width), bf16),
+            pltpu.VMEM((n, sub, 2 * hd), f32),
+            pltpu.VMEM((n, sub, 2 * hd), f32),
+            pltpu.VMEM((rows, 3 * lw), f32),
+            pltpu.VMEM((rows, 3 * lw), f32),
+            pltpu.VMEM((n, sub, lw), bf16),
+            pltpu.VMEM((n, sub, 2 * lw), bf16),
+            pltpu.VMEM((n, sub, 2 * lw), bf16),
+            pltpu.VMEM((n, sub, lw), bf16),
+            pltpu.VMEM((n, halo_sub, 2 * lw), bf16),
+            pltpu.VMEM((n, sub, lw), bf16),
+            pltpu.VMEM((n, 8, LANES), f32),
+            pltpu.VMEM((n, sub, lw), bf16),
+            pltpu.VMEM((n, 8, LANES), f32),
+            pltpu.VMEM((4, rows, lw), bf16),
+            dma((6,)),
+            dma((n,)), dma((n,)),
+            dma((n,)), dma((n,)), dma, dma, dma((n,)), dma((n,)),
+            dma((n,)), dma((n,)), dma((n,)), dma((n,)), dma((n,)), dma((n,)),
+            dma((3,)), dma((3,)),
+            dma, dma,
+            dma((n,)), dma((n,)), dma((n,)), dma((n,)),
+            dma((2,)), dma((2,)), dma, dma, dma((2,)), dma((2,)),
+        ],
+        compiler_params=pltpu.CompilerParams(
+            collective_id=0, has_side_effects=True, vmem_limit_bytes=60 * 1024 * 1024
+        ),
+    )(
+        hidden, norm_gain.astype(f32).reshape(4, 1, width), query_gain, key_gain,
+        w_query, w_key, w_value, w_out, table,
+    )
+
+
 def solution(mesh):
+    split = mesh.shape["sp"] == MIDDLE_DILATION and mesh.shape["tp"] == 4
+    chosen = local_by_class if split else local
     placed = (
         P(("grp", "sp"), "tp"),
         P(),
@@ -187,7 +548,7 @@
         P("tp", None),
     )
     return jax.shard_map(
-        local,
+        chosen,
         mesh=mesh,
         in_specs=placed,
         out_specs=(P(("grp", "sp"), "tp"), P(("grp", "sp"), "tp")),

time: 136 us -> 49.4 us (0.36)
  the two profiles are of different devices: /device:TPU:17 before, /device:TPU:1 now
where the time goes in v1:
time: 49.4 us; the launch traced here: 49.1 us
  Pallas kernels  43.8 us (89%)
  local copies, waits for them, and re-layouts  3.38 us (7%)
  other arithmetic  1.29 us (3%)
  between operations  0.64 us (1%)
    pallas_call x1, Pallas kernels, local_by_class(): pl.pallas_call(class_kernel, out_shape=(jax.ShapeDtypeStruct((rows, w_out...  43.8 us
    unnamed x1, local copies, waits for them, and re-layouts  1.77 us
    pallas_call x1, local copies, waits for them, and re-layouts, local_by_class(): pl.pallas_call(class_kernel, out_shape=(jax.ShapeDtypeStruct((rows, w_out...  1.61 us
    reshape x1, other arithmetic, local_by_class(): norm_gain.astype(f32).reshape(4, 1, width)  1.29 us

profile of v1, /device:TPU:1, one launch (start us, length us, event | category | flops | bytes accessed | tf_op | source)
XLA Modules:
  0.0 49.1 jit_solution(14557911802877423751)
XLA Ops:
  0.6 1.3 %reshape.11 = f32[2048]{0:T(1024)} convert(bf16[2048]{0:T(1024)(128)(2,1)} %param.10) | non-fusion elementwise | flops 2048 | bytes 12288 | tf_op jit(solution)/shard_map/reshape | solution.py:532
  1.9 43.8 %shard_map.104 = (bf16[384,512]{1,0:T(8,128)(2,1)}, f32[384,2]{1,0:T(8,128)}) custom-call(bf16[384,512]{1,0:T(8,128)(2,1)} %hid_ref.1, f32[4,1,512]{2,1,0:T(1,128)} %bitcast.1, f32[2,128]{1,0:T(2,128)} %qgain_ref.1, f32[2,128]{1,0:T(2,128)} %kgain_ref.1, bf16[2048,256]{1,0:T(8,128)(2,1)} %wq_ref.1, bf16[2048,256]{1,0:T(8,128)(2,1)} %wk_ref.1, ...), custom_call_target="tpu_custom_call" | custom-call | tf_op jit(solution)/shard_map/pallas_call | solution.py:492
  45.8 1.6 %copy.11 = f32[384,2]{0,1:T(2,128)} copy(f32[384,2]{1,0:T(8,128)} %get-tuple-element.3) | data formatting | bytes 6144 | tf_op jit(solution)/shard_map/pallas_call | solution.py:492
  47.4 1.8 %copy.13 = bf16[384,512]{1,0:T(8,128)(2,1)} copy(bf16[384,512]{1,0:T(8,128)(2,1)} %get-tuple-element.6) | data formatting | bytes 786432

commit v2 on v1

--- a/solution.py
+++ b/solution.py
@@ -196,7 +196,7 @@
     hid_ref, gain_ref, qgain_ref, kgain_ref, wq_ref, wk_ref, wv_ref, wo_ref, table_ref,
     mixed_ref, total_ref,
     hb, hc, wall, wo, tb, tc, acc_b, acc_c, q_b, kv_b, kv_c, q_c, halo, oc, lsend, ro, rl, at,
-    loc, zs, zr, axs, axr, acs, acr, afs, afr, cxs, cxr, ccs, ccr, cfs, cfr,
+    gain, loc, zs, zr, axs, axr, acs, acr, afs, afr, cxs, cxr, ccs, ccr, cfs, cfr,
     wos, wor, hs, hr, rs, rr, ls, lr, gxs, gxr, gcs, gcr, gfs, gfr,
 ):
     f32, bf16 = jnp.float32, jnp.bfloat16
@@ -248,6 +248,10 @@
 
     square = (rows, rows)
     to_class = (row_of(iota(square, 0), sub) == iota(square, 1)).astype(f32).astype(bf16)
+    flat_gain = gain_ref[...].astype(f32)
+    for j in range(flat_gain.shape[0]):
+        each = width // LANES
+        gain[j // each, :, (j % each) * LANES : (j % each + 1) * LANES] = flat_gain[j : j + 1]
     permuted = jnp.dot(to_class, hid_ref[...], preferred_element_type=f32).astype(bf16)
     hb[p] = permuted.reshape(n, sub, width)
     hc[p, s] = hb[p, s]
@@ -279,7 +283,7 @@
 
     def chunk(source, q):
         raw = source[q].reshape(rows, width).astype(f32)
-        scaled = (raw * gain_ref[q]).astype(bf16)
+        scaled = (raw * gain[q]).astype(bf16)
         w = wall[pl.ds(pl.multiple_of(q * width, LANES), width), :]
         return jnp.dot(scaled, w, preferred_element_type=f32), jnp.sum(raw * raw, axis=1, keepdims=True)
 
@@ -452,7 +456,9 @@
     middle = rest.astype(bf16)
     low = (rest - middle.astype(f32)).astype(bf16)
     ordered = sum(jnp.dot(from_class, x, preferred_element_type=f32) for x in (high, middle, low))
-    total_ref[...] = ordered[:, :heads]
+    for j in range(rows // LANES):
+        block = slice(j * LANES, (j + 1) * LANES)
+        total_ref[:, block] = jnp.transpose(ordered[block])[:heads]
 
     result = jnp.dot(at[p], wo[p], preferred_element_type=f32)
     for copy in w_sends:
@@ -489,11 +495,11 @@
     vmem = pl.BlockSpec(memory_space=pltpu.VMEM)
     anyspace = pl.BlockSpec(memory_space=pl.ANY)
     dma = pltpu.SemaphoreType.DMA
-    return pl.pallas_call(
+    mixed, total = pl.pallas_call(
         class_kernel,
         out_shape=(
-            jax.ShapeDtypeStruct((rows, w_out.shape[1] // 4), bf16),
-            jax.ShapeDtypeStruct((rows, heads), f32),
+            pltpu.VMEM((rows, w_out.shape[1] // 4), bf16),
+            pltpu.VMEM((heads, rows), f32),
         ),
         in_specs=[vmem] * 4 + [anyspace] * 5,
         out_specs=(vmem, vmem),
@@ -516,6 +522,7 @@
             pltpu.VMEM((n, sub, lw), bf16),
             pltpu.VMEM((n, 8, LANES), f32),
             pltpu.VMEM((4, rows, lw), bf16),
+            pltpu.VMEM((4, 1, width), f32),
             dma((6,)),
             dma((n,)), dma((n,)),
             dma((n,)), dma((n,)), dma, dma, dma((n,)), dma((n,)),
@@ -529,9 +536,10 @@
             collective_id=0, has_side_effects=True, vmem_limit_bytes=60 * 1024 * 1024
         ),
     )(
-        hidden, norm_gain.astype(f32).reshape(4, 1, width), query_gain, key_gain,
+        hidden, norm_gain.reshape(-1, LANES), query_gain, key_gain,
         w_query, w_key, w_value, w_out, table,
     )
+    return mixed, total.T
 
 
 def solution(mesh):

time: 49.4 us -> 45.3 us (0.917)
  local copies, waits for them, and re-layouts: 3.38 us -> 1.33 us
  other arithmetic: 1.29 us -> 0 us
  Pallas kernels: 43.8 us -> 43.2 us
    pallas_call x1 -> x0, local copies, waits for them, and re-layouts: 1.61 us -> none  [local_by_class(): pl.pallas_call(class_kernel, out_shape=(jax.ShapeDtypeStruct((rows, w_out...]
    reshape x1 -> x0, other arithmetic: 1.29 us -> none  [local_by_class(): norm_gain.astype(f32).reshape(4, 1, width)]
    pallas_call x1, Pallas kernels: 43.8 us -> 43.2 us  [local_by_class(): pl.pallas_call(class_kernel, out_shape=(pltpu.VMEM((rows, w_out.shape[1]...]
    unnamed x1 -> x2, local copies, waits for them, and re-layouts: 1.77 us -> 1.33 us
where the time goes in v2:
time: 45.3 us; the launch traced here: 45.1 us
  Pallas kernels  43.2 us (95%)
  local copies, waits for them, and re-layouts  1.33 us (3%)
  between operations  0.64 us (1%)
    pallas_call x1, Pallas kernels, local_by_class(): pl.pallas_call(class_kernel, out_shape=(pltpu.VMEM((rows, w_out.shape[1]...  43.2 us
    unnamed x2, local copies, waits for them, and re-layouts  1.33 us

profile of v2, /device:TPU:1, one launch (start us, length us, event | category | flops | bytes accessed | tf_op | source)
XLA Modules:
  0.0 45.1 jit_solution(14348984924241755329)
XLA Ops:
  0.6 43.2 %shard_map.104 = (bf16[384,512]{1,0:T(8,128)(2,1)S(1)}, f32[2,384]{1,0:T(2,128)S(1)}) custom-call(bf16[384,512]{1,0:T(8,128)(2,1)} %hid_ref.1, bf16[16,128]{1,0:T(8,128)(2,1)} %bitcast.3, f32[2,128]{1,0:T(2,128)} %qgain_ref.1, f32[2,128]{1,0:T(2,128)} %kgain_ref.1, bf16[2048,256]{1,0:T(8,128)(2,1)} %wq_ref.1, bf16[2048,256]{1,0:T(8,128)(2,1)} %wk_ref.1, ...), custom_call_target="tpu_custom_call" | custom-call | tf_op jit(solution)/shard_map/pallas_call | solution.py:498
  43.8 0.7 %copy.13 = bf16[384,512]{1,0:T(8,128)(2,1)} copy(bf16[384,512]{1,0:T(8,128)(2,1)S(1)} %get-tuple-element.6) | data formatting | bytes 786432
  44.5 0.6 %copy.14 = f32[384,2]{0,1:T(2,128)} copy(f32[384,2]{0,1:T(2,128)S(1)} %bitcast.2) | data formatting | bytes 6144

commit v3 on v2

--- a/solution.py
+++ b/solution.py
@@ -195,12 +195,13 @@
 def class_kernel(
     hid_ref, gain_ref, qgain_ref, kgain_ref, wq_ref, wk_ref, wv_ref, wo_ref, table_ref,
     mixed_ref, total_ref,
-    hb, hc, wall, wo, tb, tc, acc_b, acc_c, q_b, kv_b, kv_c, q_c, halo, oc, lsend, ro, rl, at,
-    gain, loc, zs, zr, axs, axr, acs, acr, afs, afr, cxs, cxr, ccs, ccr, cfs, cfr,
-    wos, wor, hs, hr, rs, rr, ls, lr, gxs, gxr, gcs, gcr, gfs, gfr,
+    hid, gain_in, qgain, kgain, hb, hc, wall, wo, tb, tc, acc_b, acc_c, q_b, kv_b, kv_c, q_c,
+    halo, oc, lsend, ro, rl, near_out, near_log, all_log, at, gain,
+    loc, zs, zr, axs, axr, acs, acr, afs, afr, cxs, cxr, ccs, ccr, cfs, cfr,
+    wos, wor, wfs, wfr, hs, hr, rs, rr, ls, lr, gxs, gxr, gcs, gcr, gfs, gfr,
 ):
     f32, bf16 = jnp.float32, jnp.bfloat16
-    s, p = lax.axis_index("sp"), lax.axis_index("tp")
+    g, s, p = lax.axis_index("grp"), lax.axis_index("sp"), lax.axis_index("tp")
     n = MIDDLE_DILATION
     rows, width = hid_ref.shape
     sub = rows // n
@@ -211,23 +212,27 @@
     core = p + 1 - 2 * lax.rem(p, 2)
     xp = lax.rem(p + 2, 4)
     diag = lax.rem(core + 2, 4)
-
-    def tp_copy(src, dst, ss, sr, q):
+    order = (1, 3, 2)
+
+    def copy_to(axis, src, dst, ss, sr, q):
         return pltpu.make_async_remote_copy(
-            src_ref=src, dst_ref=dst, send_sem=ss, recv_sem=sr, device_id={"tp": q}, device_id_type=MESH
+            src_ref=src, dst_ref=dst, send_sem=ss, recv_sem=sr, device_id={axis: q}, device_id_type=MESH
         )
 
-    def sp_copy(src, dst, ss, sr, q):
-        return pltpu.make_async_remote_copy(
-            src_ref=src, dst_ref=dst, send_sem=ss, recv_sem=sr, device_id={"sp": q}, device_id_type=MESH
-        )
-
+    tp_copy = functools.partial(copy_to, "tp")
+    sp_copy = functools.partial(copy_to, "sp")
+    load_hid = pltpu.make_async_copy(hid_ref, hid, loc.at[6])
+    load_hid.start()
     barrier = pltpu.get_barrier_semaphore()
     for q in (core, xp, diag):
         pl.semaphore_signal(barrier, inc=1, device_id={"tp": q}, device_id_type=MESH)
     for k in range(1, n):
         pl.semaphore_signal(barrier, inc=1, device_id={"sp": lax.rem(s + k, n)}, device_id_type=MESH)
+    pl.semaphore_signal(barrier, inc=1, device_id={"grp": 1 - g}, device_id_type=MESH)
     loads = [
+        pltpu.make_async_copy(gain_ref, gain_in, loc.at[7]),
+        pltpu.make_async_copy(qgain_ref, qgain, loc.at[8]),
+        pltpu.make_async_copy(kgain_ref, kgain, loc.at[9]),
         pltpu.make_async_copy(wq_ref, wall.at[:, pl.ds(0, lw)], loc.at[0]),
         pltpu.make_async_copy(wk_ref, wall.at[:, pl.ds(lw, lw)], loc.at[1]),
         pltpu.make_async_copy(wv_ref, wall.at[:, pl.ds(2 * lw, lw)], loc.at[2]),
@@ -248,14 +253,10 @@
 
     square = (rows, rows)
     to_class = (row_of(iota(square, 0), sub) == iota(square, 1)).astype(f32).astype(bf16)
-    flat_gain = gain_ref[...].astype(f32)
-    for j in range(flat_gain.shape[0]):
-        each = width // LANES
-        gain[j // each, :, (j % each) * LANES : (j % each + 1) * LANES] = flat_gain[j : j + 1]
-    permuted = jnp.dot(to_class, hid_ref[...], preferred_element_type=f32).astype(bf16)
+    load_hid.wait()
+    permuted = jnp.dot(to_class, hid[...], preferred_element_type=f32).astype(bf16)
     hb[p] = permuted.reshape(n, sub, width)
-    hc[p, s] = hb[p, s]
-    pl.semaphore_wait(barrier, 3 + n - 1)
+    pl.semaphore_wait(barrier, 3 + n)
 
     sends = []
 
@@ -264,34 +265,43 @@
         sends.append(copy)
         return copy
 
-    za = [None] + [
-        go(sp_copy(hb.at[p, lax.rem(s + k, n)], hc.at[p, s], zs.at[k], zr.at[k], lax.rem(s + k, n)))
-        for k in range(1, n)
-    ]
+    za = {}
+    for k in order:
+        to = lax.rem(s + k, n)
+        za[k] = go(sp_copy(hb.at[p, to], hc.at[p, s], zs.at[k], zr.at[k], to))
     ax = [go(tp_copy(hb.at[p, i], hb.at[p, i], axs.at[i], axr.at[i], xp)) for i in range(n)]
     ac = go(tp_copy(hb.at[p], hb.at[p], acs, acr, core))
 
     block_of = [lax.rem(s + n - k, n) for k in range(n)]
-    cx, cc = [], []
+    cx, cc, cf = {}, {}, {}
 
     def spread(k):
         piece = hc.at[p, block_of[k]]
-        cx.append(go(tp_copy(piece, piece, cxs.at[k], cxr.at[k], xp)))
-        cc.append(go(tp_copy(piece, piece, ccs.at[k], ccr.at[k], core)))
-
-    spread(0)
-
-    def chunk(source, q):
-        raw = source[q].reshape(rows, width).astype(f32)
+        cx[k] = go(tp_copy(piece, piece, cxs.at[k], cxr.at[k], xp))
+        cc[k] = go(tp_copy(piece, piece, ccs.at[k], ccr.at[k], core))
+
+    for load in loads:
+        load.wait()
+    flat_gain = gain_in[...].astype(f32)
+    for j in range(flat_gain.shape[0]):
+        each = width // LANES
+        gain[j // each, :, (j % each) * LANES : (j % each + 1) * LANES] = flat_gain[j : j + 1]
+
+    def chunk(raw, q):
+        raw = raw.astype(f32)
         scaled = (raw * gain[q]).astype(bf16)
         w = wall[pl.ds(pl.multiple_of(q * width, LANES), width), :]
         return jnp.dot(scaled, w, preferred_element_type=f32), jnp.sum(raw * raw, axis=1, keepdims=True)
 
-    for load in loads:
-        load.wait()
-    acc_b[...], sq_b = chunk(hb, p)
+    def chunk_b(q):
+        return chunk(hb[q].reshape(rows, width), q)
+
+    def chunk_c(k, q):
+        return chunk(hb[q, s] if k == 0 else hc[q, block_of[k]], q)
+
+    acc_b[...], sq_b = chunk_b(p)
     ac.wait_recv()
-    prod, more = chunk(hb, core)
+    prod, more = chunk_b(core)
     acc_b[...] += prod
     sq_b += more
 
@@ -300,36 +310,49 @@
         ax[i].wait_recv()
         af.append(go(tp_copy(hb.at[xp, i], hb.at[xp, i], afs.at[i], afr.at[i], core)))
         if i >= 1:
-            za[i].wait_recv()
-            spread(i)
-    w_sends = []
-    for j, q in enumerate((core, xp, diag)):
-        w_sends.append(
-            go(tp_copy(wo_ref.at[:, pl.ds(pl.multiple_of(q * width, LANES), width)], wo.at[p], wos.at[j], wor.at[j], q))
-        )
-
-    prod, more = chunk(hb, xp)
+            za[order[i - 1]].wait_recv()
+            spread(order[i - 1])
+    half = lw // 2
+    mine = pl.ds(pl.multiple_of(g * half, 8), half)
+    w_sends = [
+        go(tp_copy(wo_ref.at[:, pl.ds(pl.multiple_of(core * width, LANES), width)], wo.at[p], wos.at[0], wor.at[0], core))
+    ]
+    for j, q in ((1, xp), (2, diag)):
+        w_sends.append(go(tp_copy(
+            wo_ref.at[mine, pl.ds(pl.multiple_of(q * width, LANES), width)], wo.at[p, mine], wos.at[j], wor.at[j], q
+        )))
+
+    prod, more = chunk_b(xp)
     acc_b[...] += prod
     sq_b += more
     for copy in af:
         copy.wait_recv()
-    prod, more = chunk(hb, diag)
+    prod, more = chunk_b(diag)
     sq_b += more
 
-    def finish(acc, sq, table, q_out, kv_out):
+    def finish(acc, sq, table, put_q, put_kv):
         raw = acc * lax.rsqrt(sq / (width * 4) + EPSILON)
-        table = table[...].reshape(rows, 2 * hd)
         cosine, sine = table[:, :hd], table[:, hd:]
         for h in range(heads):
-            for start, gains, out in ((0, qgain_ref, q_out), (lw, kgain_ref, kv_out)):
+            for start, gains, put in ((0, qgain, put_q), (lw, kgain, put_kv)):
                 x = raw[:, start + h * hd : start + (h + 1) * hd]
                 x = x * lax.rsqrt(jnp.mean(x * x, axis=-1, keepdims=True) + EPSILON)
                 x = x * gains[pl.ds(h, 1), :]
                 x = x * cosine + pltpu.roll(x, hd // 2, 1) * sine
-                out[:, :, h * hd : (h + 1) * hd] = x.astype(bf16).reshape(n, sub, hd)
-        kv_out[:, :, lw:] = raw[:, 2 * lw :].astype(bf16).reshape(n, sub, lw)
-
-    finish(acc_b[...] + prod, sq_b, tb, q_b, kv_b)
+                put(slice(h * hd, (h + 1) * hd), x.astype(bf16))
+        put_kv(slice(lw, 2 * lw), raw[:, 2 * lw :].astype(bf16))
+
+    def put_all(ref):
+        def put(cols, x):
+            ref[:, :, cols] = x.reshape(n, sub, x.shape[1])
+        return put
+
+    def put_block(ref, b):
+        def put(cols, x):
+            ref[b, :, cols] = x
+        return put
+
+    finish(acc_b[...] + prod, sq_b, tb[...].reshape(rows, 2 * hd), put_all(q_b), put_all(kv_b))
     halo_send = sp_copy(kv_b.at[:, pl.ds(sub - halo_sub, halo_sub), :], halo, hs, hr, lax.rem(s + 1, n))
 
     @pl.when(s < n - 1)
@@ -340,26 +363,36 @@
     def _():
         halo[...] = jnp.zeros_like(halo)
 
-    cf = []
-    for k in range(n):
+    def finish_c(k, acc, sq):
+        prod, more = chunk_c(k, diag)
+        b = block_of[k]
+        finish(acc + prod, sq + more, tc[b], put_block(q_c, b), put_block(kv_c, b))
+
+    acc_0, sq_0 = chunk_c(0, p)
+    for q in (core, xp):
+        prod, more = chunk_c(0, q)
+        acc_0 += prod
+        sq_0 += more
+    finish_c(0, acc_0, sq_0)
+    before, squares = None, {}
+    for k in order:
+        cc[k].wait_recv()
+        part, squares[k] = chunk_c(k, p)
+        prod, more = chunk_c(k, core)
+        part += prod
+        squares[k] += more
         cx[k].wait_recv()
         piece = hc.at[xp, block_of[k]]
-        cf.append(go(tp_copy(piece, piece, cfs.at[k], cfr.at[k], core)))
-        if k == n - 2:
-            for copy in cc:
-                copy.wait_recv()
-            prod, sq_c = chunk(hc, p)
-            prod2, more = chunk(hc, core)
-            acc_c[...] = prod + prod2
-            sq_c += more
-    prod, more = chunk(hc, xp)
-    acc_c[...] += prod
-    sq_c += more
-    for copy in cf:
-        copy.wait_recv()
-    prod, more = chunk(hc, diag)
-    sq_c += more
-    finish(acc_c[...] + prod, sq_c, tc, q_c, kv_c)
+        cf[k] = go(tp_copy(piece, piece, cfs.at[k], cfr.at[k], core))
+        prod, more = chunk_c(k, xp)
+        squares[k] += more
+        acc_c[k] = part + prod
+        if before is not None:
+            cf[before].wait_recv()
+            finish_c(before, acc_c[before], squares[before])
+        before = k
+    cf[before].wait_recv()
+    finish_c(before, acc_c[before], squares[before])
 
     def attend(q, k, v, bias):
         score = lax.dot_general(q, k, (((1,), (1,)), ((), ())), preferred_element_type=f32)
@@ -379,6 +412,7 @@
     ).astype(f32)
     lane = iota((rows, LANES), 1)
     logs = jnp.zeros((rows, LANES), f32)
+    back = {k: [] for k in order}
     for h in range(heads):
         cols = slice(h * hd, (h + 1) * hd)
         vcols = slice(lw + h * hd, lw + (h + 1) * hd)
@@ -386,19 +420,18 @@
             q_c[:, :, cols].reshape(rows, hd), kv_c[:, :, cols].reshape(rows, hd),
             kv_c[:, :, vcols].reshape(rows, hd), bias_c,
         )
-        oc[:, :, cols] = out.astype(bf16).reshape(n, sub, hd)
+        oc[h] = out.astype(bf16).reshape(n, sub, hd)
         logs = jnp.where(lane == h, lse, logs)
+        for k in order:
+            to = lax.rem(s + k, n)
+            back[k].append(go(sp_copy(oc.at[h, to], ro.at[h, s], rs.at[h, k], rr.at[h, k], to)))
     pad = LANES - sub
     for b in range(n):
         part = jnp.concatenate([logs[b * sub : (b + 1) * sub], jnp.zeros((pad, LANES), f32)], axis=0)
         lsend[b] = jnp.transpose(part)[:8]
-    back, back_l = [], []
-    for k in range(1, n):
+    for k in order:
         to = lax.rem(s + k, n)
-        back.append(go(sp_copy(oc.at[to], ro.at[s], rs.at[k], rr.at[k], to)))
-        back_l.append(go(sp_copy(lsend.at[to], rl.at[s], ls.at[k], lr.at[k], to)))
-    ro[s] = oc[s]
-    rl[s] = lsend[s]
+        back[k].append(go(sp_copy(lsend.at[to], rl.at[s], ls.at[k], lr.at[k], to)))
 
     @pl.when(s > 0)
     def _():
@@ -411,46 +444,60 @@
     behind = row_of(iota(wide, 0), sub) - key_row
     ok = (behind >= 0) & (behind <= KEYS_BEHIND) & (key_row + s * rows >= 0)
     bias_b = jnp.where(ok, 0.0, -jnp.inf).astype(f32)
-    near_parts = []
+    logs = jnp.zeros((rows, LANES), f32)
     for h in range(heads):
         cols = slice(h * hd, (h + 1) * hd)
         vcols = slice(lw + h * hd, lw + (h + 1) * hd)
-        near_parts.append(attend(
+        out, lse = attend(
             q_b[:, :, cols].reshape(rows, hd),
             jnp.concatenate([kv_b[:, :, cols].reshape(rows, hd), halo[:, :, cols].reshape(halo_rows, hd)], axis=0),
             jnp.concatenate([kv_b[:, :, vcols].reshape(rows, hd), halo[:, :, vcols].reshape(halo_rows, hd)], axis=0),
             bias_b,
-        ))
-
-    for copy in back + back_l:
-        copy.wait_recv()
-    far_logs = jnp.concatenate(
-        [
-            jnp.transpose(jnp.concatenate([rl[i], jnp.zeros((LANES - 8, LANES), f32)], axis=0))[:sub]
-            for i in range(n)
-        ],
-        axis=0,
-    )
-    logs = jnp.zeros((rows, LANES), f32)
-    mixed_heads = []
-    for h in range(heads):
-        out, lse = near_parts[h]
-        far_lse = far_logs[:, h : h + 1]
-        far_out = ro[:, :, h * hd : (h + 1) * hd].reshape(rows, hd).astype(f32)
-        top = jnp.maximum(lse, far_lse)
-        e_near, e_far = jnp.exp(lse - top), jnp.exp(far_lse - top)
-        both = e_near + e_far
-        logs = jnp.where(lane == h, top + jnp.log(both), logs)
-        mixed_heads.append(((e_near * out + e_far * far_out) / both).astype(bf16))
-    attended = jnp.concatenate(mixed_heads, axis=1)
+        )
+        near_out[h] = out.reshape(n, sub, hd)
+        logs = jnp.where(lane == h, lse, logs)
+    near_log[...] = logs.reshape(n, sub, LANES)
+
+    wf = []
+    for j, q in ((1, xp), (2, diag)):
+        w_sends[j].wait_recv()
+        wf.append(go(copy_to("grp", wo.at[q, mine], wo.at[q, mine], wfs.at[j - 1], wfr.at[j - 1], 1 - g)))
+
+    gx, gc, gf = {}, {}, {}
+
+    def merge(k):
+        b = block_of[k]
+        received = lsend[s] if k == 0 else rl[b]
+        far_log = jnp.transpose(jnp.concatenate([received, jnp.zeros((LANES - 8, LANES), f32)], axis=0))[:sub]
+        logs = jnp.zeros((sub, LANES), f32)
+        for h in range(heads):
+            lse = near_log[b][:, h : h + 1]
+            far_lse = far_log[:, h : h + 1]
+            far_out = (oc[h, s] if k == 0 else ro[h, b]).astype(f32)
+            top = jnp.maximum(lse, far_lse)
+            e_near, e_far = jnp.exp(lse - top), jnp.exp(far_lse - top)
+            both = e_near + e_far
+            logs = jnp.where(lane[:sub] == h, top + jnp.log(both), logs)
+            at[p, b, :, h * hd : (h + 1) * hd] = ((e_near * near_out[h, b] + e_far * far_out) / both).astype(bf16)
+        all_log[b] = logs
+        piece = at.at[p, b]
+        gx[k] = go(tp_copy(piece, piece, gxs.at[k], gxr.at[k], xp))
+        gc[k] = go(tp_copy(piece, piece, gcs.at[k], gcr.at[k], core))
+
+    def forward(k):
+        gx[k].wait_recv()
+        piece = at.at[xp, block_of[k]]
+        gf[k] = go(tp_copy(piece, piece, gfs.at[k], gfr.at[k], core))
+
+    merge(0)
+    for k, ready in zip(order, (None, 0, order[0])):
+        for copy in back[k]:
+            copy.wait_recv()
+        merge(k)
+        if ready is not None:
+            forward(ready)
     from_class = (iota(square, 0) == row_of(iota(square, 1), sub)).astype(f32).astype(bf16)
-    at[p] = jnp.dot(from_class, attended, preferred_element_type=f32).astype(bf16)
-    half = rows // 2
-    gx = [
-        go(tp_copy(at.at[p, pl.ds(i * half, half)], at.at[p, pl.ds(i * half, half)], gxs.at[i], gxr.at[i], xp))
-        for i in range(2)
-    ]
-    gc = go(tp_copy(at.at[p], at.at[p], gcs, gcr, core))
+    logs = all_log[...].reshape(rows, LANES)
     high = logs.astype(bf16)
     rest = logs - high.astype(f32)
     middle = rest.astype(bf16)
@@ -460,21 +507,23 @@
         block = slice(j * LANES, (j + 1) * LANES)
         total_ref[:, block] = jnp.transpose(ordered[block])[:heads]
 
-    result = jnp.dot(at[p], wo[p], preferred_element_type=f32)
-    for copy in w_sends:
+    def product(q):
+        return jnp.dot(at[q].reshape(rows, lw), wo[q], preferred_element_type=f32)
+
+    result = product(p)
+    forward(order[1])
+    w_sends[0].wait_recv()
+    for k in range(n):
+        gc[k].wait_recv()
+    result += product(core)
+    for copy in wf:
         copy.wait_recv()
-    gc.wait_recv()
-    result += jnp.dot(at[core], wo[core], preferred_element_type=f32)
-    gf = []
-    for i in range(2):
-        gx[i].wait_recv()
-        piece = at.at[xp, pl.ds(i * half, half)]
-        gf.append(go(tp_copy(piece, piece, gfs.at[i], gfr.at[i], core)))
-    result += jnp.dot(at[xp], wo[xp], preferred_element_type=f32)
-    for copy in gf:
-        copy.wait_recv()
-    result += jnp.dot(at[diag], wo[diag], preferred_element_type=f32)
-    mixed_ref[...] = result.astype(bf16)
+    forward(order[2])
+    result += product(xp)
+    for k in range(n):
+        gf[k].wait_recv()
+    result += product(diag)
+    mixed_ref[...] = jnp.dot(from_class, result.astype(bf16), preferred_element_type=f32).astype(bf16)
     for copy in sends:
         copy.wait_send()
 
@@ -501,9 +550,13 @@
             pltpu.VMEM((rows, w_out.shape[1] // 4), bf16),
             pltpu.VMEM((heads, rows), f32),
         ),
-        in_specs=[vmem] * 4 + [anyspace] * 5,
+        in_specs=[anyspace] * 9,
         out_specs=(vmem, vmem),
         scratch_shapes=[
+            pltpu.VMEM((rows, width), bf16),
+            pltpu.VMEM((4 * width // LANES, LANES), bf16),
+            pltpu.VMEM((heads, hd), f32),
+            pltpu.VMEM((heads, hd), f32),
             pltpu.VMEM((4, n, sub, width), bf16),
             pltpu.VMEM((4, n, sub, width), bf16),
             pltpu.VMEM((4 * width, 3 * lw), bf16),
@@ -511,26 +564,29 @@
             pltpu.VMEM((n, sub, 2 * hd), f32),
             pltpu.VMEM((n, sub, 2 * hd), f32),
             pltpu.VMEM((rows, 3 * lw), f32),
-            pltpu.VMEM((rows, 3 * lw), f32),
+            pltpu.VMEM((n, sub, 3 * lw), f32),
             pltpu.VMEM((n, sub, lw), bf16),
             pltpu.VMEM((n, sub, 2 * lw), bf16),
             pltpu.VMEM((n, sub, 2 * lw), bf16),
             pltpu.VMEM((n, sub, lw), bf16),
             pltpu.VMEM((n, halo_sub, 2 * lw), bf16),
-            pltpu.VMEM((n, sub, lw), bf16),
+            pltpu.VMEM((heads, n, sub, hd), bf16),
             pltpu.VMEM((n, 8, LANES), f32),
-            pltpu.VMEM((n, sub, lw), bf16),
+            pltpu.VMEM((heads, n, sub, hd), bf16),
             pltpu.VMEM((n, 8, LANES), f32),
-            pltpu.VMEM((4, rows, lw), bf16),
+            pltpu.VMEM((heads, n, sub, hd), f32),
+            pltpu.VMEM((n, sub, LANES), f32),
+            pltpu.VMEM((n, sub, LANES), f32),
+            pltpu.VMEM((4, n, sub, lw), bf16),
             pltpu.VMEM((4, 1, width), f32),
-            dma((6,)),
+            dma((10,)),
             dma((n,)), dma((n,)),
             dma((n,)), dma((n,)), dma, dma, dma((n,)), dma((n,)),
             dma((n,)), dma((n,)), dma((n,)), dma((n,)), dma((n,)), dma((n,)),
-            dma((3,)), dma((3,)),
+            dma((3,)), dma((3,)), dma((2,)), dma((2,)),
             dma, dma,
-            dma((n,)), dma((n,)), dma((n,)), dma((n,)),
-            dma((2,)), dma((2,)), dma, dma, dma((2,)), dma((2,)),
+            dma((heads, n)), dma((heads, n)), dma((n,)), dma((n,)),
+            dma((n,)), dma((n,)), dma((n,)), dma((n,)), dma((n,)), dma((n,)),
         ],
         compiler_params=pltpu.CompilerParams(
             collective_id=0, has_side_effects=True, vmem_limit_bytes=60 * 1024 * 1024
@@ -543,7 +599,7 @@
 
 
 def solution(mesh):
-    split = mesh.shape["sp"] == MIDDLE_DILATION and mesh.shape["tp"] == 4
+    split = (mesh.shape["grp"], mesh.shape["sp"], mesh.shape["tp"]) == (2, MIDDLE_DILATION, 4)
     chosen = local_by_class if split else local
     placed = (
         P(("grp", "sp"), "tp"),

time: 45.3 us -> 40.1 us (0.89)
  Pallas kernels: 43.2 us -> 38 us
    pallas_call x1, Pallas kernels: 43.2 us -> 38 us  [local_by_class(): pl.pallas_call(class_kernel, out_shape=(pltpu.VMEM((rows, w_out.shape[1]...]
where the time goes in v3:
time: 40.1 us; the launch traced here: 40 us
  Pallas kernels  38 us (95%)
  local copies, waits for them, and re-layouts  1.33 us (3%)
  between operations  0.64 us (2%)
    pallas_call x1, Pallas kernels, local_by_class(): pl.pallas_call(class_kernel, out_shape=(pltpu.VMEM((rows, w_out.shape[1]...  38 us
    unnamed x2, local copies, waits for them, and re-layouts  1.33 us

profile of v3, /device:TPU:1, one launch (start us, length us, event | category | flops | bytes accessed | tf_op | source)
XLA Modules:
  0.0 40.0 jit_solution(13905005507512421162)
XLA Ops:
  0.6 38.0 %shard_map.104 = (bf16[384,512]{1,0:T(8,128)(2,1)S(1)}, f32[2,384]{1,0:T(2,128)S(1)}) custom-call(bf16[384,512]{1,0:T(8,128)(2,1)} %hid_ref.1, bf16[16,128]{1,0:T(8,128)(2,1)} %bitcast.3, f32[2,128]{1,0:T(2,128)} %qgain_ref.1, f32[2,128]{1,0:T(2,128)} %kgain_ref.1, bf16[2048,256]{1,0:T(8,128)(2,1)} %wq_ref.1, bf16[2048,256]{1,0:T(8,128)(2,1)} %wk_ref.1, ...), custom_call_target="tpu_custom_call" | custom-call | tf_op jit(solution)/shard_map/pallas_call | solution.py:547
  38.6 0.7 %copy.13 = bf16[384,512]{1,0:T(8,128)(2,1)} copy(bf16[384,512]{1,0:T(8,128)(2,1)S(1)} %get-tuple-element.6) | data formatting | bytes 786432
  39.4 0.6 %copy.14 = f32[384,2]{0,1:T(2,128)} copy(f32[384,2]{0,1:T(2,128)S(1)} %bitcast.2) | data formatting | bytes 6144

commit v4 on v3

--- a/solution.py
+++ b/solution.py
@@ -196,9 +196,8 @@
     hid_ref, gain_ref, qgain_ref, kgain_ref, wq_ref, wk_ref, wv_ref, wo_ref, table_ref,
     mixed_ref, total_ref,
     hid, gain_in, qgain, kgain, hb, hc, wall, wo, tb, tc, acc_b, acc_c, q_b, kv_b, kv_c, q_c,
-    halo, oc, lsend, ro, rl, near_out, near_log, all_log, at, gain,
-    loc, zs, zr, axs, axr, acs, acr, afs, afr, cxs, cxr, ccs, ccr, cfs, cfr,
-    wos, wor, wfs, wfr, hs, hr, rs, rr, ls, lr, gxs, gxr, gcs, gcr, gfs, gfr,
+    halo, oc, lsend, ro, rl, near_out, near_log, all_log, at, gain, drain,
+    loc, sent, zr, axr, acr, afr, cxr, ccr, cfr, wor, wfr, hs, hr, rr, lr, gxr, gcr, gfr,
 ):
     f32, bf16 = jnp.float32, jnp.bfloat16
     g, s, p = lax.axis_index("grp"), lax.axis_index("sp"), lax.axis_index("tp")
@@ -212,7 +211,8 @@
     core = p + 1 - 2 * lax.rem(p, 2)
     xp = lax.rem(p + 2, 4)
     diag = lax.rem(core + 2, 4)
-    order = (1, 3, 2)
+    order = (1, 2, 3)
+    block_of = [s, s + 1 - 2 * lax.rem(s, 2), 2 - s // 2, 3 - 3 * (s // 2)]
 
     def copy_to(axis, src, dst, ss, sr, q):
         return pltpu.make_async_remote_copy(
@@ -221,7 +221,7 @@
 
     tp_copy = functools.partial(copy_to, "tp")
     sp_copy = functools.partial(copy_to, "sp")
-    load_hid = pltpu.make_async_copy(hid_ref, hid, loc.at[6])
+    load_hid = pltpu.make_async_copy(hid_ref, hid, loc.at[1])
     load_hid.start()
     barrier = pltpu.get_barrier_semaphore()
     for q in (core, xp, diag):
@@ -230,16 +230,16 @@
         pl.semaphore_signal(barrier, inc=1, device_id={"sp": lax.rem(s + k, n)}, device_id_type=MESH)
     pl.semaphore_signal(barrier, inc=1, device_id={"grp": 1 - g}, device_id_type=MESH)
     loads = [
-        pltpu.make_async_copy(gain_ref, gain_in, loc.at[7]),
-        pltpu.make_async_copy(qgain_ref, qgain, loc.at[8]),
-        pltpu.make_async_copy(kgain_ref, kgain, loc.at[9]),
-        pltpu.make_async_copy(wq_ref, wall.at[:, pl.ds(0, lw)], loc.at[0]),
-        pltpu.make_async_copy(wk_ref, wall.at[:, pl.ds(lw, lw)], loc.at[1]),
-        pltpu.make_async_copy(wv_ref, wall.at[:, pl.ds(2 * lw, lw)], loc.at[2]),
-        pltpu.make_async_copy(table_ref.at[s], tb, loc.at[3]),
-        pltpu.make_async_copy(table_ref.at[:, s], tc, loc.at[4]),
+        pltpu.make_async_copy(gain_ref, gain_in, loc.at[0]),
+        pltpu.make_async_copy(qgain_ref, qgain, loc.at[2]),
+        pltpu.make_async_copy(kgain_ref, kgain, loc.at[3]),
+        pltpu.make_async_copy(wq_ref, wall.at[:, pl.ds(0, lw)], loc.at[4]),
+        pltpu.make_async_copy(wk_ref, wall.at[:, pl.ds(lw, lw)], loc.at[5]),
+        pltpu.make_async_copy(wv_ref, wall.at[:, pl.ds(2 * lw, lw)], loc.at[6]),
+        pltpu.make_async_copy(table_ref.at[s], tb, loc.at[7]),
+        pltpu.make_async_copy(table_ref.at[:, s], tc, loc.at[8]),
         pltpu.make_async_copy(
-            wo_ref.at[:, pl.ds(pl.multiple_of(p * width, LANES), width)], wo.at[p], loc.at[5]
+            wo_ref.at[:, pl.ds(pl.multiple_of(p * width, LANES), width)], wo.at[p], loc.at[9]
         ),
     ]
     for load in loads:
@@ -262,23 +262,22 @@
 
     def go(copy):
         copy.start()
-        sends.append(copy)
+        sends.append(math.prod(copy.src_ref.shape) * copy.src_ref.dtype.itemsize)
         return copy
 
-    za = {}
     for k in order:
-        to = lax.rem(s + k, n)
-        za[k] = go(sp_copy(hb.at[p, to], hc.at[p, s], zs.at[k], zr.at[k], to))
-    ax = [go(tp_copy(hb.at[p, i], hb.at[p, i], axs.at[i], axr.at[i], xp)) for i in range(n)]
-    ac = go(tp_copy(hb.at[p], hb.at[p], acs, acr, core))
-
-    block_of = [lax.rem(s + n - k, n) for k in range(n)]
+        to = block_of[k]
+        go(sp_copy(hb.at[p, to], hc.at[p, s], sent, zr.at[s], to))
+    piece_of = [lax.rem(s + k, n) for k in range(n)]
+    ax = [go(tp_copy(hb.at[p, i], hb.at[p, i], sent, axr.at[j], xp)) for j, i in enumerate(piece_of)]
+    ac = go(tp_copy(hb.at[p], hb.at[p], sent, acr, core))
+
     cx, cc, cf = {}, {}, {}
 
     def spread(k):
         piece = hc.at[p, block_of[k]]
-        cx[k] = go(tp_copy(piece, piece, cxs.at[k], cxr.at[k], xp))
-        cc[k] = go(tp_copy(piece, piece, ccs.at[k], ccr.at[k], core))
+        cx[k] = go(tp_copy(piece, piece, sent, cxr.at[k], xp))
+        cc[k] = go(tp_copy(piece, piece, sent, ccr.at[k], core))
 
     for load in loads:
         load.wait()
@@ -296,37 +295,51 @@
     def chunk_b(q):
         return chunk(hb[q].reshape(rows, width), q)
 
-    def chunk_c(k, q):
-        return chunk(hb[q, s] if k == 0 else hc[q, block_of[k]], q)
-
     acc_b[...], sq_b = chunk_b(p)
     ac.wait_recv()
     prod, more = chunk_b(core)
     acc_b[...] += prod
     sq_b += more
 
-    af = []
-    for i in range(n):
-        ax[i].wait_recv()
-        af.append(go(tp_copy(hb.at[xp, i], hb.at[xp, i], afs.at[i], afr.at[i], core)))
-        if i >= 1:
-            za[order[i - 1]].wait_recv()
-            spread(order[i - 1])
+    for j, i in enumerate(piece_of):
+        ax[j].wait_recv()
+        go(tp_copy(hb.at[xp, i], hb.at[xp, i], sent, afr, core))
+        if j >= 1:
+            source = block_of[order[j - 1]]
+            sp_copy(hb.at[p, source], hc.at[p, source], sent, zr.at[source], source).wait_recv()
+            spread(order[j - 1])
     half = lw // 2
     mine = pl.ds(pl.multiple_of(g * half, 8), half)
     w_sends = [
-        go(tp_copy(wo_ref.at[:, pl.ds(pl.multiple_of(core * width, LANES), width)], wo.at[p], wos.at[0], wor.at[0], core))
+        go(tp_copy(wo_ref.at[:, pl.ds(pl.multiple_of(core * width, LANES), width)], wo.at[p], sent, wor.at[0], core))
     ]
     for j, q in ((1, xp), (2, diag)):
         w_sends.append(go(tp_copy(
-            wo_ref.at[mine, pl.ds(pl.multiple_of(q * width, LANES), width)], wo.at[p, mine], wos.at[j], wor.at[j], q
+            wo_ref.at[mine, pl.ds(pl.multiple_of(q * width, LANES), width)], wo.at[p, mine], sent, wor.at[j], q
         )))
 
     prod, more = chunk_b(xp)
     acc_b[...] += prod
     sq_b += more
-    for copy in af:
-        copy.wait_recv()
+    def pieces(ks, q):
+        return chunk(jnp.concatenate([hb[q, s] if k == 0 else hc[q, block_of[k]] for k in ks], axis=0), q)
+
+    def close_pieces(ks):
+        for k in ks:
+            if k != 0:
+                cc[k].wait_recv()
+        first, squares = pieces(ks, p)
+        prod, more = pieces(ks, core)
+        return first + prod, squares + more
+
+    def cross(k):
+        cx[k].wait_recv()
+        piece = hc.at[xp, block_of[k]]
+        cf[k] = go(tp_copy(piece, piece, sent, cfr.at[k], core))
+
+    acc_c[0], sq_0 = close_pieces((0, 1))
+    cross(1)
+    tp_copy(hb.at[diag], hb.at[diag], sent, afr, core).wait_recv()
     prod, more = chunk_b(diag)
     sq_b += more
 
@@ -363,36 +376,27 @@
     def _():
         halo[...] = jnp.zeros_like(halo)
 
-    def finish_c(k, acc, sq):
-        prod, more = chunk_c(k, diag)
-        b = block_of[k]
-        finish(acc + prod, sq + more, tc[b], put_block(q_c, b), put_block(kv_c, b))
-
-    acc_0, sq_0 = chunk_c(0, p)
-    for q in (core, xp):
-        prod, more = chunk_c(0, q)
-        acc_0 += prod
-        sq_0 += more
-    finish_c(0, acc_0, sq_0)
-    before, squares = None, {}
-    for k in order:
-        cc[k].wait_recv()
-        part, squares[k] = chunk_c(k, p)
-        prod, more = chunk_c(k, core)
-        part += prod
-        squares[k] += more
-        cx[k].wait_recv()
-        piece = hc.at[xp, block_of[k]]
-        cf[k] = go(tp_copy(piece, piece, cfs.at[k], cfr.at[k], core))
-        prod, more = chunk_c(k, xp)
-        squares[k] += more
-        acc_c[k] = part + prod
-        if before is not None:
-            cf[before].wait_recv()
-            finish_c(before, acc_c[before], squares[before])
-        before = k
-    cf[before].wait_recv()
-    finish_c(before, acc_c[before], squares[before])
+    def finish_c(ks, acc, sq):
+        prod, more = pieces(ks, diag)
+        acc, sq = acc + prod, sq + more
+        for j, k in enumerate(ks):
+            part, b = slice(j * sub, (j + 1) * sub), block_of[k]
+            finish(acc[part], sq[part], tc[b], put_block(q_c, b), put_block(kv_c, b))
+
+    prod, more = pieces((0, 1), xp)
+    acc_c[0] += prod
+    sq_0 += more
+    cf[1].wait_recv()
+    finish_c((0, 1), acc_c[0], sq_0)
+    cross(2)
+    acc_c[1], sq_1 = close_pieces((2, 3))
+    cross(3)
+    prod, more = pieces((2, 3), xp)
+    acc_c[1] += prod
+    sq_1 += more
+    cf[2].wait_recv()
+    cf[3].wait_recv()
+    finish_c((2, 3), acc_c[1], sq_1)
 
     def attend(q, k, v, bias):
         score = lax.dot_general(q, k, (((1,), (1,)), ((), ())), preferred_element_type=f32)
@@ -412,7 +416,6 @@
     ).astype(f32)
     lane = iota((rows, LANES), 1)
     logs = jnp.zeros((rows, LANES), f32)
-    back = {k: [] for k in order}
     for h in range(heads):
         cols = slice(h * hd, (h + 1) * hd)
         vcols = slice(lw + h * hd, lw + (h + 1) * hd)
@@ -422,16 +425,16 @@
         )
         oc[h] = out.astype(bf16).reshape(n, sub, hd)
         logs = jnp.where(lane == h, lse, logs)
-        for k in order:
-            to = lax.rem(s + k, n)
-            back[k].append(go(sp_copy(oc.at[h, to], ro.at[h, s], rs.at[h, k], rr.at[h, k], to)))
+        for k in order[::-1]:
+            to = block_of[k]
+            go(sp_copy(oc.at[h, to], ro.at[s, h], sent, rr.at[s], to))
     pad = LANES - sub
     for b in range(n):
         part = jnp.concatenate([logs[b * sub : (b + 1) * sub], jnp.zeros((pad, LANES), f32)], axis=0)
         lsend[b] = jnp.transpose(part)[:8]
-    for k in order:
-        to = lax.rem(s + k, n)
-        back[k].append(go(sp_copy(lsend.at[to], rl.at[s], ls.at[k], lr.at[k], to)))
+    for k in order[::-1]:
+        to = block_of[k]
+        go(sp_copy(lsend.at[to], rl.at[s], sent, lr.at[s], to))
 
     @pl.when(s > 0)
     def _():
@@ -458,11 +461,6 @@
         logs = jnp.where(lane == h, lse, logs)
     near_log[...] = logs.reshape(n, sub, LANES)
 
-    wf = []
-    for j, q in ((1, xp), (2, diag)):
-        w_sends[j].wait_recv()
-        wf.append(go(copy_to("grp", wo.at[q, mine], wo.at[q, mine], wfs.at[j - 1], wfr.at[j - 1], 1 - g)))
-
     gx, gc, gf = {}, {}, {}
 
     def merge(k):
@@ -473,7 +471,7 @@
         for h in range(heads):
             lse = near_log[b][:, h : h + 1]
             far_lse = far_log[:, h : h + 1]
-            far_out = (oc[h, s] if k == 0 else ro[h, b]).astype(f32)
+            far_out = (oc[h, s] if k == 0 else ro[b, h]).astype(f32)
             top = jnp.maximum(lse, far_lse)
             e_near, e_far = jnp.exp(lse - top), jnp.exp(far_lse - top)
             both = e_near + e_far
@@ -481,18 +479,23 @@
             at[p, b, :, h * hd : (h + 1) * hd] = ((e_near * near_out[h, b] + e_far * far_out) / both).astype(bf16)
         all_log[b] = logs
         piece = at.at[p, b]
-        gx[k] = go(tp_copy(piece, piece, gxs.at[k], gxr.at[k], xp))
-        gc[k] = go(tp_copy(piece, piece, gcs.at[k], gcr.at[k], core))
+        gx[k] = go(tp_copy(piece, piece, sent, gxr.at[k], xp))
+        gc[k] = go(tp_copy(piece, piece, sent, gcr, core))
 
     def forward(k):
         gx[k].wait_recv()
         piece = at.at[xp, block_of[k]]
-        gf[k] = go(tp_copy(piece, piece, gfs.at[k], gfr.at[k], core))
+        gf[k] = go(tp_copy(piece, piece, sent, gfr, core))
 
     merge(0)
+    wf = []
+    for j, q in ((1, xp), (2, diag)):
+        w_sends[j].wait_recv()
+        wf.append(go(copy_to("grp", wo.at[q, mine], wo.at[q, mine], sent, wfr.at[j - 1], 1 - g)))
     for k, ready in zip(order, (None, 0, order[0])):
-        for copy in back[k]:
-            copy.wait_recv()
+        b = block_of[k]
+        sp_copy(ro.at[b], ro.at[b], sent, rr.at[b], b).wait_recv()
+        sp_copy(rl.at[b], rl.at[b], sent, lr.at[b], b).wait_recv()
         merge(k)
         if ready is not None:
             forward(ready)
@@ -513,19 +516,17 @@
     result = product(p)
     forward(order[1])
     w_sends[0].wait_recv()
-    for k in range(n):
-        gc[k].wait_recv()
+    tp_copy(at.at[core], at.at[core], sent, gcr, core).wait_recv()
     result += product(core)
     for copy in wf:
         copy.wait_recv()
     forward(order[2])
     result += product(xp)
-    for k in range(n):
-        gf[k].wait_recv()
+    tp_copy(at.at[diag], at.at[diag], sent, gfr, core).wait_recv()
     result += product(diag)
     mixed_ref[...] = jnp.dot(from_class, result.astype(bf16), preferred_element_type=f32).astype(bf16)
-    for copy in sends:
-        copy.wait_send()
+    assert sum(sends) == drain.shape[0] * LANES * 4
+    tp_copy(drain, drain, sent, acr, core).wait_send()
 
     @pl.when(s < n - 1)
     def _():
@@ -541,6 +542,7 @@
     halo_sub = KEYS_BEHIND // n
     bf16, f32 = jnp.bfloat16, jnp.float32
     table = jnp.asarray(rotary_table(n, sub, hd))
+    sent_bytes = 2 * (24 * sub * width + 3 * lw * width + 3 * sub * lw + 12 * sub * lw) + 3 * 8 * LANES * 4
     vmem = pl.BlockSpec(memory_space=pltpu.VMEM)
     anyspace = pl.BlockSpec(memory_space=pl.ANY)
     dma = pltpu.SemaphoreType.DMA
@@ -564,7 +566,7 @@
             pltpu.VMEM((n, sub, 2 * hd), f32),
             pltpu.VMEM((n, sub, 2 * hd), f32),
             pltpu.VMEM((rows, 3 * lw), f32),
-            pltpu.VMEM((n, sub, 3 * lw), f32),
+            pltpu.VMEM((2, 2 * sub, 3 * lw), f32),
             pltpu.VMEM((n, sub, lw), bf16),
             pltpu.VMEM((n, sub, 2 * lw), bf16),
             pltpu.VMEM((n, sub, 2 * lw), bf16),
@@ -572,21 +574,16 @@
             pltpu.VMEM((n, halo_sub, 2 * lw), bf16),
             pltpu.VMEM((heads, n, sub, hd), bf16),
             pltpu.VMEM((n, 8, LANES), f32),
-            pltpu.VMEM((heads, n, sub, hd), bf16),
+            pltpu.VMEM((n, heads, sub, hd), bf16),
             pltpu.VMEM((n, 8, LANES), f32),
             pltpu.VMEM((heads, n, sub, hd), f32),
             pltpu.VMEM((n, sub, LANES), f32),
             pltpu.VMEM((n, sub, LANES), f32),
             pltpu.VMEM((4, n, sub, lw), bf16),
             pltpu.VMEM((4, 1, width), f32),
-            dma((10,)),
-            dma((n,)), dma((n,)),
-            dma((n,)), dma((n,)), dma, dma, dma((n,)), dma((n,)),
-            dma((n,)), dma((n,)), dma((n,)), dma((n,)), dma((n,)), dma((n,)),
-            dma((3,)), dma((3,)), dma((2,)), dma((2,)),
-            dma, dma,
-            dma((heads, n)), dma((heads, n)), dma((n,)), dma((n,)),
-            dma((n,)), dma((n,)), dma((n,)), dma((n,)), dma((n,)), dma((n,)),
+            pltpu.VMEM((sent_bytes // (4 * LANES), LANES), f32),
+            dma((10,)), dma, dma((n,)), dma((n,)), dma, dma, dma((n,)), dma((n,)), dma((n,)),
+            dma((3,)), dma((2,)), dma, dma, dma((n,)), dma((n,)), dma((n,)), dma, dma,
         ],
         compiler_params=pltpu.CompilerParams(
             collective_id=0, has_side_effects=True, vmem_limit_bytes=60 * 1024 * 1024

time: 40.1 us -> 38.7 us (0.965)
  Pallas kernels: 38 us -> 36.5 us
    pallas_call x1, Pallas kernels: 38 us -> 36.5 us  [local_by_class(): pl.pallas_call(class_kernel, out_shape=(pltpu.VMEM((rows, w_out.shape[1]...]
where the time goes in v4:
time: 38.7 us; the launch traced here: 38.5 us
  Pallas kernels  36.5 us (94%)
  local copies, waits for them, and re-layouts  1.33 us (3%)
  between operations  0.64 us (2%)
    pallas_call x1, Pallas kernels, local_by_class(): pl.pallas_call(class_kernel, out_shape=(pltpu.VMEM((rows, w_out.shape[1]...  36.5 us
    unnamed x2, local copies, waits for them, and re-layouts  1.33 us

profile of v4, /device:TPU:1, one launch (start us, length us, event | category | flops | bytes accessed | tf_op | source)
XLA Modules:
  0.0 38.5 jit_solution(2317533163601098509)
XLA Ops:
  0.6 36.5 %shard_map.104 = (bf16[384,512]{1,0:T(8,128)(2,1)S(1)}, f32[2,384]{1,0:T(2,128)S(1)}) custom-call(bf16[384,512]{1,0:T(8,128)(2,1)} %hid_ref.1, bf16[16,128]{1,0:T(8,128)(2,1)} %bitcast.3, f32[2,128]{1,0:T(2,128)} %qgain_ref.1, f32[2,128]{1,0:T(2,128)} %kgain_ref.1, bf16[2048,256]{1,0:T(8,128)(2,1)} %wq_ref.1, bf16[2048,256]{1,0:T(8,128)(2,1)} %wk_ref.1, ...), custom_call_target="tpu_custom_call" | custom-call | tf_op jit(solution)/shard_map/pallas_call | solution.py:549
  37.1 0.7 %copy.13 = bf16[384,512]{1,0:T(8,128)(2,1)} copy(bf16[384,512]{1,0:T(8,128)(2,1)S(1)} %get-tuple-element.6) | data formatting | bytes 786432
  37.9 0.6 %copy.14 = f32[384,2]{0,1:T(2,128)} copy(f32[384,2]{0,1:T(2,128)S(1)} %bitcast.2) | data formatting | bytes 6144
